TPU v7x, 256 devices: a whole 4x4x8 slice. The times are simulated.
256 devices in a mesh: sp: 64 (over z, x, core), tp: 4 (over y).
Axes of the slice: x: 4, y: 4, z: 8, core: 2. Of those that a mesh axis runs over, the one named last changes fastest.
Arguments:
- incoming_residual_stream: bfloat16 [32768, 2048], P(('sp', 'tp')), may hold values from -6 to 6
- result_valve: bfloat16 [32768, 2048], P('sp', 'tp'), may hold values from -6 to 6
- channel_feed_matrix: bfloat16 [32768, 2048], P('sp', 'tp'), may hold values from -6 to 6
- memory_feed_matrix: bfloat16 [32768, 512], P('sp', 'tp'), may hold values from -6 to 6
- memory_query_matrix: bfloat16 [32768, 512], P('sp', 'tp'), may hold values from -6 to 6
- unsoftened_deltas: float32 [32768, 32], P('sp', 'tp'), may hold values from -2.7 to 2.7
- delta_offset: float32 [32], P('tp'), may hold values from -4.5 to -3.5
- channel_fading_speed: float32 [32], P('tp'), as said below
- extra_log_fading: float32 [32768, 32], P('sp', 'tp'), may hold values from -0.7 to 0
- bypass_factor: float32 [32], P('tp'), may hold values from 0.1 to 1.9
- channel_feed_kernel: bfloat16 [4, 2048], P(None, 'tp'), may hold values from -3 to 3
- memory_feed_kernel: bfloat16 [4, 512], P(None, 'tp'), may hold values from -3 to 3
- memory_query_kernel: bfloat16 [4, 512], P(None, 'tp'), may hold values from -3 to 3
- cluster_scaling_vector: float32 [2048], P('tp'), may hold values from 0.1 to 1.9
- mixer_result_matrix: bfloat16 [2048, 2048], P('tp'), may hold values from -0.125 to 0.125
- initial_scaling_vector: float32 [2048], replicated, may hold values from 0.1 to 1.9
- valve_matrix: bfloat16 [2048, 5632], P('sp', 'tp'), may hold values from -0.125 to 0.125
- widen_matrix: bfloat16 [2048, 5632], P('sp', 'tp'), may hold values from -0.125 to 0.125
- shrink_matrix: bfloat16 [5632, 2048], P('tp', 'sp'), may hold values from -0.078125 to 0.078125
- valve_filter_kernel: bfloat16 [3, 5632], P(None, 'tp'), may hold values from -3.5 to 3.5
- widen_filter_kernel: bfloat16 [3, 5632], P(None, 'tp'), may hold values from -3.5 to 3.5
- latter_scaling_vector: float32 [2048], replicated, may hold values from 0.1 to 1.9
Outputs:
- layer_out: bfloat16 [32768, 2048], P(('sp', 'tp'))
Inputs may be any that keep to these rules, and one draw needn't show every extreme that they name: `channel_fading_speed`: positive.
All inputs are finite; a program needn't handle non-finite values.
Results may differ from a plain program's by a relative error of at most 0.02.
Values may be sent and summed in bfloat16 or wider, within the bound.
A program may use at most 128 MiB of HBM per device.

v0:
```python
import jax
import jax.numpy as jnp
from jax import lax
from jax.sharding import Mesh
from jax.sharding import PartitionSpec as P

HEADS = 32
HEAD_DIM = 64
GROUPS = 4
STATE = 128
CONV = 4
FCONV = 3
BLOCK = 128
SP = ("sp_0", "sp_1", "sp_2")
SP_TP = ("sp_0", "sp_1", "sp_2", "tp")


EPSILON = 1e-05
ALPHA = 2.0**0.25


def gather_turned(arrays, axis, dims):
    turned = [jnp.moveaxis(a, dim, 0) for a, dim in zip(arrays, dims)]
    both = jnp.concatenate([t.reshape(len(t), -1) for t in turned], axis=1)
    out, at, finished = (lax.all_gather(both, axis, axis=0, tiled=True), 0, [])
    for t, dim in zip(turned, dims):
        slab = out[:, at : at + t[0].size].reshape(-1, *t.shape[1:])
        finished.append(jnp.moveaxis(slab, 0, dim))
        at += t[0].size
    return tuple(finished)


def shifted(shard, axis, by):
    count = lax.axis_size(axis)
    pairs = [(i, i + by) for i in range(count) if 0 <= i + by < count]
    return lax.ppermute(shard, axis, pairs)


def neutral_like(shard, identity):
    return jax.tree.map(
        lambda part, zero: jnp.zeros_like(part) + jnp.asarray(zero, part.dtype), shard, identity
    )


def entering(shard, axes, combine, identity):
    before = start = neutral_like(shard, identity)
    total = shard
    for axis in reversed(axes):
        count, place = (lax.axis_size(axis), lax.axis_index(axis))
        pieces = jax.tree.map(
            lambda part, kind: lax.all_gather(part.astype(kind), axis),
            total,
            (jnp.bfloat16, jnp.bfloat16),
        )
        inside, total = (start, start)
        for k in range(count):
            passed = k < place
            total = combine(
                total, jax.tree.map(lambda part, own: part[k].astype(own.dtype), pieces, shard)
            )
            inside = jax.tree.map(lambda new, old: jnp.where(passed, new, old), total, inside)
        before = combine(inside, before)
    return before


def in_blocks(shard, dim, count):
    before, after = (shard.shape[:dim], shard.shape[dim + 1 :])
    return jnp.moveaxis(shard.reshape(*before, count, -1, *after), dim, 0)


def sent_and_summed(shard, axis, dim):
    count = lax.axis_size(axis)
    pieces = lax.all_to_all(in_blocks(shard, dim, count), axis, 0, 0, tiled=True)
    return jnp.sum(pieces.astype(jnp.float32), axis=0)


def joined_along(pieces, dim):
    lengths = list(pieces.shape[1:])
    lengths[dim] *= pieces.shape[0]
    return jnp.moveaxis(pieces, 0, dim).reshape(lengths)


def sent_to_all(shard, axis):
    copies = jnp.broadcast_to(shard, (lax.axis_size(axis), *shard.shape))
    return lax.all_to_all(copies, axis, split_axis=0, concat_axis=0, tiled=True)


def gathered_copies(shard, axis, dim):
    return joined_along(sent_to_all(shard, axis), dim)


def causal_conv(signal, before, tap_weights):
    tap_count = tap_weights.shape[0]
    row_count = signal.shape[0]
    padded = jnp.concatenate([before, signal], axis=0).astype(jnp.float32)
    running = jnp.zeros(signal.shape, jnp.float32)
    for tap_index in range(tap_count):
        running = (
            running
            + tap_weights[tap_index].astype(jnp.float32) * padded[tap_index : tap_index + row_count]
        )
    return running


def layer_norm(values, scales):
    row_mean = jnp.mean(values, axis=-1, keepdims=True)
    centred = values - row_mean
    spread = jnp.mean(centred * centred, axis=-1, keepdims=True)
    return centred * lax.rsqrt(spread + EPSILON) * scales


def combine_states(earlier_pair, later_pair):
    return (
        earlier_pair[0] * later_pair[1][..., None, None] + later_pair[0],
        earlier_pair[1] * later_pair[1],
    )


def chain_step(state_now, inputs):
    fresh_one, decay_one = inputs
    return (state_now * decay_one[..., None, None] + fresh_one, state_now)


def shards(
    incoming_residual_stream,
    result_valve,
    channel_feed_matrix,
    memory_feed_matrix,
    memory_query_matrix,
    unsoftened_deltas,
    delta_offset,
    channel_fading_speed,
    extra_log_fading,
    bypass_factor,
    channel_feed_kernel,
    memory_feed_kernel,
    memory_query_kernel,
    cluster_scaling_vector,
    mixer_result_matrix,
    initial_scaling_vector,
    valve_matrix,
    widen_matrix,
    shrink_matrix,
    valve_filter_kernel,
    widen_filter_kernel,
    latter_scaling_vector,
):
    row_count = channel_feed_matrix.shape[0]
    inner_here = channel_feed_matrix.shape[1]
    group_count = memory_feed_matrix.shape[1] // STATE
    group_heads = HEADS // GROUPS
    block_count = row_count // BLOCK
    gate_whole, up_whole, down_whole = gather_turned(
        (valve_matrix, widen_matrix, shrink_matrix), SP, (0, 0, 1)
    )
    rim_rows = CONV - 1
    rim_x, rim_b, rim_c = shifted(
        (
            channel_feed_matrix[row_count - rim_rows :],
            memory_feed_matrix[row_count - rim_rows :],
            memory_query_matrix[row_count - rim_rows :],
        ),
        SP,
        1,
    )
    x_act = jax.nn.silu(causal_conv(channel_feed_matrix, rim_x, channel_feed_kernel)).astype(
        jnp.bfloat16
    )
    b_act = jax.nn.silu(causal_conv(memory_feed_matrix, rim_b, memory_feed_kernel)).astype(
        jnp.bfloat16
    )
    c_act = jax.nn.silu(causal_conv(memory_query_matrix, rim_c, memory_query_kernel)).astype(
        jnp.bfloat16
    )
    channel_delta_amount = jax.nn.softplus(unsoftened_deltas + delta_offset[None, :])
    log_fading_amount = extra_log_fading - channel_fading_speed[None, :] * channel_delta_amount
    x_heads = x_act.astype(jnp.float32).reshape(row_count, group_count, group_heads, HEAD_DIM)
    x_scaled = (
        x_heads * channel_delta_amount.reshape(row_count, group_count, group_heads)[..., None]
    )
    b_full = b_act.astype(jnp.float32).reshape(row_count, group_count, STATE)
    c_full = c_act.astype(jnp.float32).reshape(row_count, group_count, STATE)
    decay_full = log_fading_amount.reshape(row_count, group_count, group_heads)
    x_blk = x_scaled.reshape(block_count, BLOCK, group_count, group_heads, HEAD_DIM)
    b_blk = b_full.reshape(block_count, BLOCK, group_count, STATE)
    c_blk = c_full.reshape(block_count, BLOCK, group_count, STATE)
    b_narrow = b_act.reshape(block_count, BLOCK, group_count, STATE)
    c_narrow = c_act.reshape(block_count, BLOCK, group_count, STATE)
    decay_blk = decay_full.reshape(block_count, BLOCK, group_count, group_heads)
    cum_decay = jnp.cumsum(decay_blk, axis=1)
    causal = jnp.tril(jnp.ones((BLOCK, BLOCK), dtype=bool))
    between = cum_decay[:, :, None] - cum_decay[:, None, :]
    lag = jnp.exp(jnp.where(causal[None, :, :, None, None], between, -jnp.inf))
    affinity = jnp.einsum("blgn,bsgn->blsg", c_narrow, b_narrow, preferred_element_type=jnp.float32)
    mixing = affinity[..., None] * lag
    within = jnp.einsum("blsgh,bsghp->blghp", mixing, x_blk)
    to_end = jnp.exp(cum_decay[:, -1:] - cum_decay)
    fresh = jnp.einsum("blgn,blghp->bghpn", b_blk, x_blk * to_end[..., None])
    block_decay = jnp.exp(cum_decay[:, -1])
    initial = jnp.zeros((group_count, group_heads, HEAD_DIM, STATE), jnp.float32)
    local_end, earlier = lax.scan(chain_step, initial, (fresh, block_decay))
    carried = jnp.einsum("blgn,bghpn->blghp", c_blk, earlier) * jnp.exp(cum_decay)[..., None]
    from_start = jnp.cumsum(decay_full, axis=0)
    incoming, _ = entering(
        (local_end, jnp.exp(from_start[-1])),
        SP,
        combine_states,
        (jnp.zeros_like(local_end), jnp.ones_like(from_start[-1])),
    )
    arriving = jnp.einsum("tgn,ghpn->tghp", c_full, incoming) * jnp.exp(from_start)[..., None]
    y_heads = (within + carried).reshape(row_count, group_count, group_heads, HEAD_DIM) + arriving
    y_heads = y_heads + bypass_factor.reshape(group_count, group_heads)[None, :, :, None] * x_heads
    gated = y_heads.reshape(row_count, group_count, group_heads * HEAD_DIM)
    gated = gated * jax.nn.silu(result_valve.astype(jnp.float32)).reshape(
        row_count, group_count, group_heads * HEAD_DIM
    )
    gated = gated * lax.rsqrt(jnp.mean(gated * gated, axis=-1, keepdims=True) + EPSILON)
    y_norm = (gated.reshape(row_count, inner_here) * cluster_scaling_vector[None, :]).astype(
        jnp.bfloat16
    )
    mixer = sent_and_summed(
        jnp.dot(y_norm, mixer_result_matrix, preferred_element_type=jnp.float32).astype(
            jnp.bfloat16
        ),
        "tp",
        0,
    )
    normed_own = layer_norm(
        ALPHA * incoming_residual_stream.astype(jnp.float32) + mixer, initial_scaling_vector
    ).astype(jnp.bfloat16)
    normed_all = gathered_copies(normed_own, "tp", 0)
    gate_sum = jnp.dot(normed_all, gate_whole, preferred_element_type=jnp.float32)
    up_sum = jnp.dot(normed_all, up_whole, preferred_element_type=jnp.float32)
    gate_proj = gate_sum.astype(jnp.bfloat16)
    up_proj = up_sum.astype(jnp.bfloat16)
    ffn_rows = FCONV - 1
    rim_gate, rim_up = shifted(
        (gate_proj[row_count - ffn_rows :], up_proj[row_count - ffn_rows :]), SP, 1
    )
    gate_conv = causal_conv(gate_proj, rim_gate, valve_filter_kernel)
    up_conv = causal_conv(up_proj, rim_up, widen_filter_kernel)
    hidden = (jax.nn.silu(gate_conv) * up_conv).astype(jnp.bfloat16)
    channel_part = jnp.dot(hidden, down_whole, preferred_element_type=jnp.float32)
    channel = sent_and_summed(channel_part.astype(jnp.bfloat16), "tp", 0)
    return layer_norm(
        ALPHA * normed_own.astype(jnp.float32) + channel, latter_scaling_vector
    ).astype(jnp.bfloat16)


def solution(mesh):
    split = Mesh(mesh.devices.reshape(8, 4, 2, mesh.shape["tp"]), ("sp_0", "sp_1", "sp_2", "tp"))
    in_specs = (
        P(SP_TP, None),
        P(SP, "tp"),
        P(SP, "tp"),
        P(SP, "tp"),
        P(SP, "tp"),
        P(SP, "tp"),
        P("tp"),
        P("tp"),
        P(SP, "tp"),
        P("tp"),
        P(None, "tp"),
        P(None, "tp"),
        P(None, "tp"),
        P("tp"),
        P("tp", None),
        P(),
        P(SP, "tp"),
        P(SP, "tp"),
        P("tp", SP),
        P(None, "tp"),
        P(None, "tp"),
        P(),
    )
    out_specs = P(SP_TP, None)
    return jax.shard_map(
        shards, mesh=split, in_specs=in_specs, out_specs=out_specs, check_vma=False
    )
```

profile of v0, /device:TPU:1, one launch (start us, length us, event | category | flops | bytes accessed | tf_op | source)
XLA Modules:
  0.0 273.3 jit_solution(8756651230453433856)
XLA Ops:
  6.5 0.8 slice.239
  7.4 4.5 %collective-permute-start.1 = (bf16[3,128]{1,0:T(4,128)(2,1)S(1)}, bf16[3,128]{1,0:T(4,128)(2,1)S(1)}, u32[]{:S(2)}, u32[]{:S(2)}) collective-permute-start(bf16[3,128]{1,0:T(4,128)(2,1)S(1)} %slice.239), channel_id=1, source_target_pairs={{0,4},{4,8},{8,12},{12,16},{16,20},{20,24},{24,28},{28,32},{32,36}... | collective-permute-start | bytes 2312 | tf_op jit(solution)/shard_map/ppermute | solution.py:36
  11.9 0.7 slice.230
  12.6 1.9 collective-permute-start
  14.5 0.8 bitcast_convert_fusion.7
  15.3 1.4 slice_convert_fusion.3
  16.8 0.8 fusion.171
  17.6 1.1 reduce-window.6
  19.0 0.7 exponential_bitcast_fusion
  19.8 2.0 all_gather.29
  21.8 8.0 %all_gather.30 = bf16[4,1,8]{2,1,0:T(2,128)(2,1)S(1)} all-gather(bf16[1,1,8]{2,1,0:T(2,128)(2,1)S(1)} %multiply_convert_fusion.8), channel_id=1, replica_groups=mesh['sp_0'=8,'sp_1'=4,'sp_2'=2,'tp'=4] {'sp_1'}, dimensions={0}, use_global_device_ids=true | all-gather | bytes 80 | tf_op jit(solution)/shard_map/all_gather | solution.py:51
  31.4 0.8 fusion.175
  34.0 0.9 maximum_convert_fusion.3
  36.0 1.3 copy.70
  37.4 1.6 reshape.588
  38.9 1.8 broadcast_multiply_fusion
  41.1 5.7 %while.13 = (s32[]{:T(128)}, f32[1,8,64,128]{3,2,1,0:T(8,128)S(1)}, bf16[4,1,8,64,128]{4,3,2,1,0:T(8,128)(2,1)}, f32[4,1,8]{2,1,0:T(1,128)}, f32[4,1,8,64,128]{4,3,2,1,0:T(8,128)S(1)}, /*index=5*/s32[]{:T(128)}, s32[]{:T(128)}) while((s32[]{:T(128)}, f32[1,8,64,128]{3,2,1,0:T(8,128)S(1)}, bf16[4,1,8,64,128]{4,3,2,1,0:T(8,128)(2,1)}, ...), condition=%wide.region_2.3_spmd.clone, body=%wide.region_1.2_spmd.clone.sunk | while | flops 262147 | bytes 1179852 | solution.py:201
  41.7 0.7 bitcast_dynamic-update-slice_fusion.2
  45.9 0.7 bitcast_dynamic-update-slice_fusion.2
  46.8 4.1 %all-gather = bf16[2,8,64,128]{3,2,1,0:T(8,128)(2,1)S(1)} all-gather(bf16[1,8,64,128]{3,2,1,0:T(8,128)(2,1)S(1)} %convert_element_type.491), channel_id=2, replica_groups=mesh['sp_0'=8,'sp_1'=4,'sp_2'=2,'tp'=4] {'sp_2'}, dimensions={0}, use_global_device_ids=true | all-gather | bytes 393216 | tf_op jit(solution)/shard_map/all_gather | solution.py:51
  50.9 0.7 fusion.107
  51.6 9.9 %all_gather.34 = bf16[4,1,8,64,128]{4,3,2,1,0:T(8,128)(2,1)S(1)} all-gather(bf16[1,1,8,64,128]{4,3,2,1,0:T(8,128)(2,1)S(1)} %fusion.107), channel_id=1, replica_groups=mesh['sp_0'=8,'sp_1'=4,'sp_2'=2,'tp'=4] {'sp_1'}, dimensions={0}, use_global_device_ids=true | all-gather | bytes 655360 | tf_op jit(solution)/shard_map/all_gather | solution.py:51
  61.5 0.8 copy-done.5
  62.4 1.5 fusion.106
  64.0 1.7 pad_maximum_fusion
  65.7 3.9 %collective-permute-start.2 = (bf16[3,128]{1,0:T(4,128)(2,1)S(1)}, bf16[3,128]{1,0:T(4,128)(2,1)S(1)}, u32[]{:S(2)}, u32[]{:S(2)}) collective-permute-start(bf16[3,128]{1,0:T(4,128)(2,1)S(1)} %slice.248), channel_id=1, source_target_pairs={{0,4},{4,8},{8,12},{12,16},{16,20},{20,24},{24,28},{28,32},{32,36}... | collective-permute-start | bytes 2312 | tf_op jit(solution)/shard_map/ppermute | solution.py:36
  69.7 14.4 %all_gather.31 = bf16[8,1,8]{2,1,0:T(2,128)(2,1)S(1)} all-gather(bf16[1,1,8]{2,1,0:T(2,128)(2,1)S(1)} %multiply_convert_fusion.7), channel_id=1, replica_groups=mesh['sp_0'=8,'sp_1'=4,'sp_2'=2,'tp'=4] {'sp_0'}, dimensions={0}, use_global_device_ids=true | all-gather | bytes 144 | tf_op jit(solution)/shard_map/all_gather | solution.py:51
  85.9 0.7 copy.74
  87.3 2.1 fusion.28
  89.4 1.4 fusion.35
  90.9 1.7 copy.82
  92.5 8.7 %all-gather.4.cloned.1.call-done = bf16[8,1,8,64,128]{4,3,2,1,0:T(8,128)(2,1)} async-done(((bf16[1,1,8,64,128]{4,3,2,1,0:T(8,128)(2,1)}), bf16[8,1,8,64,128]{4,3,2,1,0:T(8,128)(2,1)}) %all-gather.4.cloned.1.call-update) | async-done | bytes 1048592 | tf_op jit(solution)/shard_map/all_gather | solution.py:51
  101.2 3.6 %fusion.33 = f32[512,1,8,64]{0,3,2,1:T(8,128)} fusion(f32[512,1,8,64]{0,1,3,2:T(1,128)} %bitcast.234, f32[512,1,8,64]{0,3,2,1:T(8,128)S(1)} %bitcast.225, f32[8]{0:T(128)} %param.33, f32[512,8]{0,1:T(8,128)} %get-tuple-element.91, bf16[8,1,8,64,128]{4,3,2,1,0:T(8,128)(2,1)} %all-gather.4.cloned.1.call-done, ...), kind=kOutput, calls=%fused_computation.41 | convolution fusion | flops 71892992 | bytes 5128750 | tf_op jit(solution)/shard_map/tgn,ghpn->tghp/dot_general | solution.py:210
  104.9 1.6 copy.87
  106.4 1.5 multiply_reduce_fusion.2
  107.9 2.5 convolution_convert_fusion
  110.4 25.8 %all_to_all.15 = bf16[4,128,2048]{2,1,0:T(8,128)(2,1)S(1)} all-to-all(bf16[4,128,2048]{2,1,0:T(8,128)(2,1)S(1)} %bitcast.229), channel_id=1, replica_groups=mesh['sp_0'=8,'sp_1'=4,'sp_2'=2,'tp'=4] {'tp'}, dimensions={0} | all-to-all | bytes 4194304 | tf_op jit(solution)/shard_map/all_to_all | solution.py:73
  137.5 1.6 broadcast_in_dim.20
  139.1 4.6 %all-to-all-start.1 = ((bf16[4,128,2048]{2,1,0:T(8,128)(2,1)}), bf16[4,128,2048]{2,1,0:T(8,128)(2,1)}, u32[]{:S(2)}, u32[]{:S(2)}) async-start(bf16[4,128,2048]{2,1,0:T(8,128)(2,1)} %broadcast_in_dim.20), calls=%async_computation.1 | async-start | bytes 4194304 | tf_op jit(solution)/shard_map/all_to_all | solution.py:85
  143.9 19.8 %all-to-all-done.1 = bf16[4,128,2048]{2,1,0:T(8,128)(2,1)} async-done(((bf16[4,128,2048]{2,1,0:T(8,128)(2,1)}), bf16[4,128,2048]{2,1,0:T(8,128)(2,1)}, u32[]{:S(2)}, u32[]{:S(2)}) %all-to-all-start.1) | async-done | bytes 2097184 | tf_op jit(solution)/shard_map/all_to_all | solution.py:85
  163.7 44.6 %all-gather.6.cloned.1.call-done = bf16[2048,4224]{1,0:T(8,128)(2,1)} async-done(((bf16[32,4224]{1,0:T(8,128)(2,1)}), bf16[2048,4224]{1,0:T(8,128)(2,1)}) %all-gather.6.cloned.1.call-update) | async-done | bytes 17301520 | tf_op jit(solution)/shard_map/all_gather | solution.py:25
  208.2 6.7 %fusion.7 = bf16[512,1408]{1,0:T(8,128)(2,1)S(1)} fusion(bf16[512,2048]{1,0:T(8,128)(2,1)} %bitcast.67, bf16[2048,4224]{1,0:T(8,128)(2,1)} %all-gather.6.cloned.1.call-done), kind=kOutput, calls=%fused_computation.12 | convolution fusion | flops 2953510912 | bytes 9306112 | tf_op jit(solution)/shard_map/dot_general | solution.py:232
  214.9 2.0 collective-permute-start.3
  217.0 6.7 %fusion.10 = bf16[512,1408]{1,0:T(8,128)(2,1)S(1)} fusion(bf16[512,2048]{1,0:T(8,128)(2,1)} %bitcast.67, bf16[2048,4224]{1,0:T(8,128)(2,1)} %all-gather.6.cloned.1.call-done), kind=kOutput, calls=%fused_computation.13 | convolution fusion | flops 2953510912 | bytes 9306112 | tf_op jit(solution)/shard_map/dot_general | solution.py:233
  223.7 2.2 collective-permute-start.4
  227.0 7.6 %fusion.13 = bf16[512,2048]{1,0:T(8,128)(2,1)S(1)} fusion(bf16[2048,4224]{1,0:T(8,128)(2,1)} %all-gather.6.cloned.1.call-done, f32[514,1408]{1,0:T(8,128)S(1)} %maximum_convert_fusion.1, f32[514,1408]{1,0:T(8,128)S(1)} %maximum_convert_fusion, f32[1408]{0:T(1024)S(1)} %get-tuple-element.77, f32[1408]{0:T(1024)S(1)} %get-tuple-element.78, ...), kind=kOutput, calls=%fused_computation.15 | convolution fusion | flops 2965372928 | bytes 25214976 | tf_op jit(solution)/shard_map/dot_general | solution.py:243
  234.7 29.8 %all_to_all.16 = bf16[4,128,2048]{2,1,0:T(8,128)(2,1)S(1)} all-to-all(bf16[4,128,2048]{2,1,0:T(8,128)(2,1)S(1)} %bitcast.228), channel_id=1, replica_groups=mesh['sp_0'=8,'sp_1'=4,'sp_2'=2,'tp'=4] {'tp'}, dimensions={0} | all-to-all | bytes 4194304 | tf_op jit(solution)/shard_map/all_to_all | solution.py:73
  265.4 1.1 multiply_convert_fusion
  (117 shorter events, 15.3 us)
Async XLA Ops:
  6.5 101.4 %copy-start = (bf16[512,2048]{1,0:T(8,128)(2,1)S(1)}, bf16[512,2048]{1,0:T(8,128)(2,1)}, u32[]{:S(2)}) copy-start(bf16[512,2048]{1,0:T(8,128)(2,1)} %param.38) | copy-start | bytes 6291460
  6.5 28.6 %copy-start.9 = (bf16[512,512]{1,0:T(8,128)(2,1)S(1)}, bf16[512,512]{1,0:T(8,128)(2,1)}, u32[]{:S(2)}) copy-start(bf16[512,512]{1,0:T(8,128)(2,1)} %param.26) | copy-start | bytes 1572868
  6.5 94.7 %all-gather.4.cloned.1.call-start = ((), (), s32[]{:S(2)}) async-start(), calls=%async_computation.3 | async-start | bytes 1179648 | tf_op jit(solution)/shard_map/all_gather | solution.py:51
  7.4 26.7 %collective-permute-start.1 = (bf16[3,128]{1,0:T(4,128)(2,1)S(1)}, bf16[3,128]{1,0:T(4,128)(2,1)S(1)}, u32[]{:S(2)}, u32[]{:S(2)}) collective-permute-start(bf16[3,128]{1,0:T(4,128)(2,1)S(1)} %slice.239), channel_id=1, source_target_pairs={{0,4},{4,8},{8,12},{12,16},{16,20},{20,24},{24,28},{28,32},{32,36}... | collective-permute-start | bytes 2312 | tf_op jit(solution)/shard_map/ppermute | solution.py:36
  12.6 22.6 %collective-permute-start = (bf16[3,512]{1,0:T(4,128)(2,1)S(1)}, bf16[3,512]{1,0:T(4,128)(2,1)S(1)}, u32[]{:S(2)}, u32[]{:S(2)}) collective-permute-start(bf16[3,512]{1,0:T(4,128)(2,1)S(1)} %slice.230), channel_id=1, source_target_pairs={{0,4},{4,8},{8,12},{12,16},{16,20},{20,24},{24,28},{28,32},{32,36}... | collective-permute-start | bytes 9224 | tf_op jit(solution)/shard_map/ppermute | solution.py:36
  29.8 5.5 %copy-start.11 = (bf16[4,1,8]{2,1,0:T(2,128)(2,1)}, bf16[4,1,8]{2,1,0:T(2,128)(2,1)S(1)}, u32[]{:S(2)}) copy-start(bf16[4,1,8]{2,1,0:T(2,128)(2,1)S(1)} %all_gather.30) | copy-start | bytes 196
  30.7 0.7 copy-start.3
  34.0 1.4 copy-start.15
  34.0 1.4 copy-start.16
  34.0 1.4 copy-start.17
  34.0 1.4 copy-start.18
  41.0 9.9 %copy-start.23 = (f32[8]{0:T(128)S(1)}, f32[8]{0:T(128)}, u32[]{:S(2)}) copy-start(f32[8]{0:T(128)} %get-tuple-element.117) | copy-start | bytes 100
  41.1 21.3 %copy-start.22 = (f32[8]{0:T(128)S(1)}, f32[8]{0:T(128)}, u32[]{:S(2)}) copy-start(f32[8]{0:T(128)} %get-tuple-element.113) | copy-start | bytes 100
  46.7 19.0 %copy-start.10 = (bf16[512,128]{1,0:T(8,128)(2,1)S(1)}, bf16[512,128]{1,0:T(8,128)(2,1)}, u32[]{:S(2)}) copy-start(bf16[512,128]{1,0:T(8,128)(2,1)} %param.28) | copy-start | bytes 393220
  46.7 22.9 %copy-start.12 = (bf16[4,1,8]{2,1,0:T(2,128)(2,1)S(1)}, bf16[4,1,8]{2,1,0:T(2,128)(2,1)}, u32[]{:S(2)}) copy-start(bf16[4,1,8]{2,1,0:T(2,128)(2,1)} %copy-done.11) | copy-start | bytes 196
  46.7 38.5 %copy-start.21 = (bf16[4,128]{1,0:T(4,128)(2,1)S(1)}, bf16[4,128]{1,0:T(4,128)(2,1)}, u32[]{:S(2)}) copy-start(bf16[4,128]{1,0:T(4,128)(2,1)} %param.36) | copy-start | bytes 3076
  46.8 39.1 %copy-start.4 = (f32[4,128,1,8]{3,2,1,0:T(1,128)S(1)}, f32[4,128,1,8]{3,2,1,0:T(1,128)}, u32[]{:S(2)}) copy-start(f32[4,128,1,8]{3,2,1,0:T(1,128)} %copy-done.3) | copy-start | bytes 49156
  46.8 39.8 %copy-start.6 = (f32[4,128,8]{2,1,0:T(8,128)S(1)}, f32[4,128,8]{2,1,0:T(8,128)}, u32[]{:S(2)}) copy-start(f32[4,128,8]{2,1,0:T(8,128)} %get-tuple-element.95) | copy-start | bytes 49156
  50.9 36.4 %copy-start.7 = (bf16[2,8,64,128]{3,2,1,0:T(8,128)(2,1)}, bf16[2,8,64,128]{3,2,1,0:T(8,128)(2,1)S(1)}, u32[]{:S(2)}) copy-start(bf16[2,8,64,128]{3,2,1,0:T(8,128)(2,1)S(1)} %all-gather) | copy-start | bytes 786436
  61.5 0.8 copy-start.5
  63.9 144.3 %all-gather.6.cloned.1.call-start = ((), (), s32[]{:S(2)}) async-start(), calls=%async_computation.4 | async-start | bytes 17571840 | tf_op jit(solution)/shard_map/all_gather | solution.py:25
  65.7 21.0 %collective-permute-start.2 = (bf16[3,128]{1,0:T(4,128)(2,1)S(1)}, bf16[3,128]{1,0:T(4,128)(2,1)S(1)}, u32[]{:S(2)}, u32[]{:S(2)}) collective-permute-start(bf16[3,128]{1,0:T(4,128)(2,1)S(1)} %slice.248), channel_id=1, source_target_pairs={{0,4},{4,8},{8,12},{12,16},{16,20},{20,24},{24,28},{28,32},{32,36}... | collective-permute-start | bytes 2312 | tf_op jit(solution)/shard_map/ppermute | solution.py:36
  89.4 11.8 %copy-start.2 = (f32[512,512]{0,1:T(8,128)S(1)}, f32[512,512]{0,1:T(8,128)}, u32[]{:S(2)}) copy-start(f32[512,512]{0,1:T(8,128)} %copy.70) | copy-start | bytes 3145732
  89.4 11.8 %copy-start.8 = (bf16[2,8,64,128]{3,2,1,0:T(8,128)(2,1)S(1)}, bf16[2,8,64,128]{3,2,1,0:T(8,128)(2,1)}, u32[]{:S(2)}) copy-start(bf16[2,8,64,128]{3,2,1,0:T(8,128)(2,1)} %copy-done.7) | copy-start | bytes 786436
  104.9 3.1 %copy-start.24 = (f32[512]{0:T(512)S(1)}, f32[512]{0:T(512)}, u32[]{:S(2)}) copy-start(f32[512]{0:T(512)} %param.37) | copy-start | bytes 6148
  110.4 26.2 %copy-start.1 = (bf16[128,2048]{1,0:T(8,128)(2,1)S(1)}, bf16[128,2048]{1,0:T(8,128)(2,1)}, u32[]{:S(2)}) copy-start(bf16[128,2048]{1,0:T(8,128)(2,1)} %param.24) | copy-start | bytes 1572868
  136.3 0.9 copy-start.19
  137.5 6.3 %copy-start.13 = (bf16[3,1408]{1,0:T(4,128)(2,1)S(1)}, bf16[3,1408]{1,0:T(4,128)(2,1)}, u32[]{:S(2)}) copy-start(bf16[3,1408]{1,0:T(4,128)(2,1)} %param.44) | copy-start | bytes 25348
  137.5 6.3 %copy-start.14 = (bf16[3,1408]{1,0:T(4,128)(2,1)S(1)}, bf16[3,1408]{1,0:T(4,128)(2,1)}, u32[]{:S(2)}) copy-start(bf16[3,1408]{1,0:T(4,128)(2,1)} %param.43) | copy-start | bytes 25348
  139.1 24.6 %all-to-all-start.1 = ((bf16[4,128,2048]{2,1,0:T(8,128)(2,1)}), bf16[4,128,2048]{2,1,0:T(8,128)(2,1)}, u32[]{:S(2)}, u32[]{:S(2)}) async-start(bf16[4,128,2048]{2,1,0:T(8,128)(2,1)} %broadcast_in_dim.20), calls=%async_computation.1 | async-start | bytes 4194304 | tf_op jit(solution)/shard_map/all_to_all | solution.py:85
  214.9 10.9 %collective-permute-start.3 = (bf16[2,1408]{1,0:T(2,128)(2,1)S(1)}, bf16[2,1408]{1,0:T(2,128)(2,1)S(1)}, u32[]{:S(2)}, u32[]{:S(2)}) collective-permute-start(bf16[2,1408]{1,0:T(2,128)(2,1)S(1)} %slice.351), channel_id=1, source_target_pairs={{0,4},{4,8},{8,12},{12,16},{16,20},{20,24},{24,28},{28,32},{32,36}... | collective-permute-start | bytes 16904 | tf_op jit(solution)/shard_map/ppermute | solution.py:36
  223.7 3.1 %collective-permute-start.4 = (bf16[2,1408]{1,0:T(2,128)(2,1)S(1)}, bf16[2,1408]{1,0:T(2,128)(2,1)S(1)}, u32[]{:S(2)}, u32[]{:S(2)}) collective-permute-start(bf16[2,1408]{1,0:T(2,128)(2,1)S(1)} %slice.356), channel_id=1, source_target_pairs={{0,4},{4,8},{8,12},{12,16},{16,20},{20,24},{24,28},{28,32},{32,36}... | collective-permute-start | bytes 16904 | tf_op jit(solution)/shard_map/ppermute | solution.py:36
  264.4 1.0 copy-start.20
Sparse Core Ops, SparseCore 0:
  64.0 37.1 all-gather.3
  103.9 104.2 all-gather.5
where the time goes:
time: 274 us; the launch traced here: 273 us
  blocking collectives  94 us (34%)
  waiting for transfers between devices  73.7 us (27%)
  matrix products  31.1 us (11%)
  other arithmetic  25.9 us (9%)
  starting transfers between devices  19.1 us (7%)
  local copies, waits for them, and re-layouts  15.4 us (6%)
  between operations  14 us (5%)
    all_to_all x2, blocking collectives, sent_and_summed(): lax.all_to_all(in_blocks(shard, dim, count), axis, 0, 0, tiled=True)  55.6 us
    all_gather x1, waiting for transfers between devices, gather_turned(): out, at, finished = (lax.all_gather(both, axis, axis=0, tiled=True), 0, [])  44.6 us
    all_gather x5, blocking collectives, entering(): lax.all_gather(part.astype(kind), axis)  38.4 us
    all_to_all x1, waiting for transfers between devices, sent_to_all(): return lax.all_to_all(copies, axis, split_axis=0, concat_axis=0, tiled=True)  19.8 us
    ppermute x5, starting transfers between devices, shifted(): return lax.ppermute(shard, axis, pairs)  14.5 us
    all_gather x1, waiting for transfers between devices, entering(): lax.all_gather(part.astype(kind), axis)  8.67 us
    dot_general x1, matrix products, shards(): jnp.dot(hidden, down_whole, preferred_element_type=jnp.float32)  7.63 us
    dot_general x1, matrix products, shards(): up_sum = jnp.dot(normed_all, up_whole, preferred_element_type=jnp.float32)  6.68 us
  transfers between devices with their start and end apart: 8, of which 4 were waited for; matrix products, arithmetic and copies ran while one was open for 15% of the time, Pallas kernels for 0%

commit v1 on v0

v1 whole, which is shorter than its diff:
```python
import jax
import jax.numpy as jnp
from jax import lax
from jax.experimental import pallas as pl
from jax.experimental.pallas import tpu as pltpu
from jax.sharding import Mesh
from jax.sharding import PartitionSpec as P

HEADS = 8
HEAD_DIM = 64
STATE = 128
BLOCK = 128
BLOCKS = 4
ROWS = BLOCK * BLOCKS
INNER = 512
D = 2048
FF = 1408
COLS = 3 * FF
NA = 1664
EPSILON = 1e-05
ALPHA = 2.0**0.25
SP = ("sp_0", "sp_1", "sp_2")
SP_TP = ("sp_0", "sp_1", "sp_2", "tp")
MESH = pl.DeviceIdType.MESH
F32 = jnp.float32
BF16 = jnp.bfloat16
NT = (((1,), (1,)), ((), ()))


def wrap(value, count):
    return lax.rem(value + 2 * count, count)


class Wire:
    def __init__(self, send_sem):
        self.send_sem = send_sem
        self.count = 0
        self.waits = []

    def send(self, src, dst, dev, recv_sem, when=None):
        copy = pltpu.make_async_remote_copy(
            src_ref=src,
            dst_ref=dst,
            send_sem=self.send_sem.at[self.count],
            recv_sem=recv_sem,
            device_id=dev,
            device_id_type=MESH,
        )
        self.count += 1
        if when is None:
            copy.start()
        else:
            pl.when(when)(copy.start)
        self.waits.append((copy, when))

    def arrive(self, dst, recv_sem, dev):
        pltpu.make_async_remote_copy(
            src_ref=dst,
            dst_ref=dst,
            send_sem=self.send_sem.at[0],
            recv_sem=recv_sem,
            device_id=dev,
            device_id_type=MESH,
        ).wait_recv()

    def finish(self):
        for copy, when in self.waits:
            if when is None:
                copy.wait_send()
            else:
                pl.when(when)(copy.wait_send)


def weight_gather(wire, wv, rsem, psem, ids):
    z, x, c, _ = ids
    cols_a, cols_b = pl.ds(0, NA), pl.ds(NA, COLS - NA)
    half, whole = (pl.ds(0, 16), pl.ds(16, 16)), pl.ds(0, 32)
    zp, zm = {"sp_0": wrap(z + 1, 8)}, {"sp_0": wrap(z - 1, 8)}
    xp, xm = {"sp_1": wrap(x + 1, 4)}, {"sp_1": wrap(x - 1, 4)}
    other = {"sp_2": 1 - c}
    xl, xr, xf = wrap(x - 1, 4), wrap(x + 1, 4), wrap(x + 2, 4)

    def piece(zz, xx, cols, rows=whole):
        return wv.at[zz, xx, c, rows, cols]

    def group(zz, rows=whole):
        return wv.at[zz, :, c, rows, cols_a]

    def send(view, dev, sem):
        wire.send(view, view, dev, sem)

    def arrive(view, sem):
        wire.arrive(view, sem, other)

    def a1(d, h):
        return rsem.at[d * 2 + h]

    def a1f(d):
        return rsem.at[4 + d]

    def a2(d, s):
        return rsem.at[6 + d * 4 + s - 1]

    def b1(d, s):
        return rsem.at[14 + d * 4 + s - 1]

    def b2(d, s):
        return rsem.at[22 + d * 8 + s]

    def b2f(d, s):
        return rsem.at[38 + d * 8 + s]

    def along_x(off):
        v = piece(wrap(z + off, 8), x, cols_b)
        send(v, xp, b2(0, off % 8))
        send(v, xm, b2(1, off % 8))
        send(v, other, psem)

    def start():
        send(piece(z, x, cols_b), zp, b1(0, 1))
        send(piece(z, x, cols_b), zm, b1(1, 1))
        send(piece(z, x, cols_a, half[0]), xp, a1(0, 0))
        send(piece(z, x, cols_a, half[1]), xm, a1(1, 1))
        send(piece(z, x, cols_a, half[1]), xp, a1(0, 1))
        send(piece(z, x, cols_a, half[0]), xm, a1(1, 0))
        along_x(0)

    def row_far():
        v = piece(z, xl, cols_a, half[0])
        arrive(v, a1(0, 0))
        send(v, xp, a1f(0))
        v = piece(z, xr, cols_a, half[1])
        arrive(v, a1(1, 1))
        send(v, xm, a1f(1))

    def row_done():
        arrive(piece(z, xl, cols_a, half[1]), a1(0, 1))
        arrive(piece(z, xr, cols_a, half[0]), a1(1, 0))
        arrive(piece(z, xf, cols_a, half[0]), a1f(0))
        arrive(piece(z, xf, cols_a, half[1]), a1f(1))
        send(group(z), zp, a2(0, 1))
        send(group(z), zm, a2(1, 1))
        send(group(z), other, psem)

    def z_piece(s):
        zl, zr = wrap(z - s, 8), wrap(z + s, 8)
        if s < 4:
            v = piece(zl, x, cols_b)
            arrive(v, b1(0, s))
            send(v if s < 3 else piece(zl, x, cols_b, half[0]), zp, b1(0, s + 1))
            v = piece(zr, x, cols_b)
            arrive(v, b1(1, s))
            send(v if s < 3 else piece(zr, x, cols_b, half[1]), zm, b1(1, s + 1))
            along_x(-s)
            along_x(s)
        else:
            arrive(piece(zl, x, cols_b, half[0]), b1(0, 4))
            arrive(piece(zl, x, cols_b, half[1]), b1(1, 4))
            along_x(4)

    def z_group(s):
        zl, zr = wrap(z - s, 8), wrap(z + s, 8)
        if s < 4:
            arrive(group(zl), a2(0, s))
            send(group(zl) if s < 3 else group(zl, half[0]), zp, a2(0, s + 1))
            arrive(group(zr), a2(1, s))
            send(group(zr) if s < 3 else group(zr, half[1]), zm, a2(1, s + 1))
            send(group(zl), other, psem)
            send(group(zr), other, psem)
        else:
            arrive(group(zl, half[0]), a2(0, 4))
            arrive(group(zl, half[1]), a2(1, 4))
            send(group(zl), other, psem)

    def x_piece(off):
        zz = wrap(z + off, 8)
        v = piece(zz, xl, cols_b)
        arrive(v, b2(0, off % 8))
        send(piece(zz, xl, cols_b, half[0]), xp, b2f(0, off % 8))
        send(v, other, psem)
        v = piece(zz, xr, cols_b)
        arrive(v, b2(1, off % 8))
        send(piece(zz, xr, cols_b, half[1]), xm, b2f(1, off % 8))
        send(v, other, psem)

    def x_far(off):
        zz = wrap(z + off, 8)
        arrive(piece(zz, xf, cols_b, half[0]), b2f(0, off % 8))
        arrive(piece(zz, xf, cols_b, half[1]), b2f(1, off % 8))
        send(piece(zz, xf, cols_b), other, psem)

    def finish():
        arrive(wv.at[pl.ds(0, 4)], psem)

    return [
        start,
        row_far,
        lambda: z_piece(1),
        row_done,
        lambda: x_piece(0),
        lambda: z_piece(2),
        lambda: (x_piece(-1), x_piece(1)),
        lambda: z_group(1),
        lambda: z_piece(3),
        lambda: (x_piece(-2), x_piece(2), x_far(0)),
        lambda: z_piece(4),
        lambda: z_group(2),
        lambda: (x_piece(-3), x_piece(3), x_far(1), x_far(-1)),
        lambda: (x_piece(4), x_far(2), x_far(-2)),
        lambda: z_group(3),
        lambda: (x_far(3), x_far(-3), x_far(4)),
        lambda: z_group(4),
        finish,
    ]


def thirds(v):
    high = v.astype(BF16)
    rest = v - high.astype(F32)
    mid = rest.astype(BF16)
    return high, mid, (rest - mid.astype(F32)).astype(BF16)


def dot(a, b):
    return jnp.dot(a, b, preferred_element_type=F32)


def exact_left(selector, v):
    return sum(dot(selector, part) for part in thirds(v))


def spread(v, onehot):
    return sum(dot(part, onehot) for part in thirds(v))


def silu(v):
    return v * (1.0 / (1.0 + jnp.exp(-v)))


def layer_norm(values, scales):
    centred = values - jnp.mean(values, axis=-1, keepdims=True)
    spread_of = jnp.mean(centred * centred, axis=-1, keepdims=True)
    return centred * lax.rsqrt(spread_of + EPSILON) * scales


def layer_kernel(
    resid,
    valve,
    x_in,
    b_in,
    c_in,
    deltas,
    offset,
    speed,
    fading,
    bypass,
    x_taps,
    b_taps,
    c_taps,
    cluster,
    w_mix,
    scale_one,
    w_gate,
    w_up,
    w_down,
    gate_taps,
    up_taps,
    scale_two,
    out,
    wv,
    x_rim,
    b_rim,
    c_rim,
    xs,
    bs,
    cs,
    cums,
    turned,
    ec,
    yw,
    states,
    decays,
    ends,
    row_ends,
    row_decay,
    row_pre,
    row_dpre,
    own_decay,
    z_state,
    z_decay,
    z_out,
    z_dout,
    z_acc,
    to_row,
    incoming,
    mix_out,
    mix_far,
    mix_in,
    nall,
    gu,
    ffn_out,
    ffn_far,
    ffn_in,
    send_sem,
    gather_sem,
    pair_sem,
    rim_sem,
    row_sem,
    z_sem,
    back_sem,
    mix_sem,
    all_sem,
    ffn_sem,
):
    ids = tuple(lax.axis_index(name) for name in SP_TP)
    z, x, c, y = ids
    rank = z * 8 + x * 2 + c
    place = x * 2 + c
    wire = Wire(send_sem)

    def rank_dev(r, tp=None):
        dev = {"sp_0": lax.div(r, 8), "sp_1": lax.div(lax.rem(r, 8), 2), "sp_2": lax.rem(r, 2)}
        if tp is not None:
            dev["tp"] = tp
        return dev

    def row_dev(p):
        return {"sp_1": lax.div(p, 2), "sp_2": lax.rem(p, 2)}

    after, before = wrap(rank + 1, 64), wrap(rank - 1, 64)
    right, left = {"tp": wrap(y + 1, 4)}, {"tp": wrap(y - 1, 4)}

    sem = pltpu.get_barrier_semaphore()
    greeted = [{"sp_0": wrap(z + k, 8)} for k in range(1, 8)]
    greeted += [row_dev(wrap(place + k, 8)) for k in range(1, 8)]
    greeted += [right, left]
    greeted += [rank_dev(before, k) for k in range(4)]
    for dev in greeted:
        pl.semaphore_signal(sem, inc=1, device_id=dev, device_id_type=MESH)

    ident = (
        lax.broadcasted_iota(jnp.int32, (32, 32), 0) == lax.broadcasted_iota(jnp.int32, (32, 32), 1)
    ).astype(BF16)
    wv[z, x, c, :, 0:FF] = w_gate[...]
    wv[z, x, c, :, FF : 2 * FF] = w_up[...]
    wv[z, x, c, :, 2 * FF :] = lax.dot_general(
        ident, w_down[...], NT, preferred_element_type=F32
    ).astype(BF16)
    pl.semaphore_wait(sem, len(greeted))

    has_next, has_last = rank < 63, rank > 0
    last = pl.ds(ROWS - 16, 16)
    for k, (src, dst) in enumerate(((x_in, x_rim), (b_in, b_rim), (c_in, c_rim))):
        wire.send(src.at[last], dst, rank_dev(after), rim_sem.at[k], when=has_next)
    gather = weight_gather(wire, wv, gather_sem, pair_sem, ids)
    gather[0]()

    rows_at = lax.broadcasted_iota(jnp.int32, (BLOCK, BLOCK), 0)
    cols_at = lax.broadcasted_iota(jnp.int32, (BLOCK, BLOCK), 1)
    causal = rows_at >= cols_at
    tril = causal.astype(BF16)
    onehot = (
        lax.broadcasted_iota(jnp.int32, (HEADS, INNER), 0)
        == lax.div(lax.broadcasted_iota(jnp.int32, (HEADS, INNER), 1), HEAD_DIM)
    ).astype(BF16)
    skip = spread(jnp.broadcast_to(bypass[...], (8, HEADS)), onehot)[0:1]
    low_lanes = lax.broadcasted_iota(jnp.int32, (BLOCK, 2 * HEAD_DIM), 1) < HEAD_DIM

    def conv_block(src, rim, taps, b):
        if b == 0:
            window = jnp.concatenate([rim[...], src[0:BLOCK]], axis=0).astype(F32)
        else:
            window = src[b * BLOCK - 16 : (b + 1) * BLOCK].astype(F32)
        weights = taps[...].astype(F32)
        total = weights[0:1] * window[13 : 13 + BLOCK]
        for k in range(1, 4):
            total = total + weights[k : k + 1] * window[13 + k : 13 + k + BLOCK]
        return silu(total)

    def local_block(b):
        span = slice(b * BLOCK, (b + 1) * BLOCK)
        x_act = conv_block(x_in, x_rim, x_taps, b).astype(BF16)
        b_act = conv_block(b_in, b_rim, b_taps, b).astype(BF16)
        xs[span] = x_act
        bs[span] = b_act
        cs[span] = conv_block(c_in, c_rim, c_taps, b).astype(BF16)
        raw = deltas[span] + offset[...]
        step = jnp.maximum(raw, 0.0) + jnp.log1p(jnp.exp(-jnp.abs(raw)))
        cum = exact_left(tril, fading[span] - speed[...] * step)
        cums[span, 0:HEADS] = cum
        cums[span, HEADS : 2 * HEADS] = step
        turned[b] = cums[span].T[0 : 2 * HEADS]
        grown = spread(jnp.exp(cum), onehot)
        ec[span] = grown
        to_end = spread(step * jnp.exp(cum[BLOCK - 1 : BLOCK] - cum), onehot)
        weighted = (x_act.astype(F32) * to_end).astype(BF16)
        states[b] = dot(b_act.astype(F32).T.astype(BF16), weighted)
        decays[b] = jnp.broadcast_to(grown[BLOCK - 1 : BLOCK], (8, INNER))

    def within_block(b):
        span = slice(b * BLOCK, (b + 1) * BLOCK)
        affinity = lax.dot_general(cs[span], bs[span], NT, preferred_element_type=F32)
        for pair in range(HEADS // 2):
            lanes = slice(pair * 128, (pair + 1) * 128)
            mixing = []
            for h in (2 * pair, 2 * pair + 1):
                between = cums[span, h : h + 1] - turned[b, h : h + 1]
                lag = jnp.exp(jnp.where(causal, between, -1e30))
                mixing.append((affinity * lag * turned[b, HEADS + h : HEADS + h + 1]).astype(BF16))
            x_pair = xs[span, lanes]
            zero = jnp.zeros_like(x_pair)
            sides = jnp.concatenate(
                [jnp.where(low_lanes, x_pair, zero), jnp.where(low_lanes, zero, x_pair)], axis=0
            )
            yw[span, lanes] = dot(jnp.concatenate(mixing, axis=1), sides) + skip[
                :, lanes
            ] * x_pair.astype(F32)

    def packed(v):
        return jnp.concatenate([v[:, k * 128 : (k + 1) * 128] for k in range(4)], axis=0)

    def unpacked(tile):
        return jnp.concatenate([tile[k : k + 1] for k in range(4)], axis=1)

    cums[...] = jnp.zeros_like(cums)
    local_block(3)
    gather[1]()
    local_block(2)
    local_block(1)

    @pl.when(has_last)
    def _():
        for k, dst in enumerate((x_rim, b_rim, c_rim)):
            wire.arrive(dst, rim_sem.at[k], rank_dev(before))

    @pl.when(jnp.logical_not(has_last))
    def _():
        for dst in (x_rim, b_rim, c_rim):
            dst[...] = jnp.zeros_like(dst)

    local_block(0)

    total = jnp.zeros((STATE, INNER), F32)
    growth = jnp.ones((1, INNER), F32)
    for b in range(BLOCKS):
        fresh, decay = states[b], decays[b, 0:1]
        states[b] = total
        decays[b] = jnp.broadcast_to(growth, (8, INNER))
        total = total * decay + fresh
        growth = growth * decay
    ends[...] = total.astype(BF16)
    own_decay[...] = jnp.zeros_like(own_decay)
    own_decay[0:4] = packed(growth)

    def sixteen(p):
        return pl.ds(pl.multiple_of(p * 16, 16), 16)

    for k in range(1, 8):
        to = wrap(place + k, 8)
        wire.send(ends.at[sixteen(to)], row_ends.at[place], row_dev(to), row_sem.at[0, k])
        wire.send(own_decay, row_decay.at[place], row_dev(to), row_sem.at[1, k])
    row_ends[place] = ends[sixteen(place), :]
    row_decay[place] = own_decay[...]
    gather[2]()
    within_block(0)
    within_block(1)
    for k in range(1, 8):
        src = wrap(place - k, 8)
        wire.arrive(row_ends.at[src], row_sem.at[0, k], row_dev(src))
        wire.arrive(row_decay.at[src], row_sem.at[1, k], row_dev(src))
    total = jnp.zeros((16, INNER), F32)
    growth = jnp.ones((1, INNER), F32)
    for q in range(8):
        decay = unpacked(row_decay[q])
        row_pre[q] = total
        row_dpre[q] = jnp.broadcast_to(growth, (8, INNER))
        total = total * decay + row_ends[q].astype(F32)
        growth = growth * decay
    z_out[...] = total.astype(BF16)
    z_dout[...] = jnp.zeros_like(z_dout)
    z_dout[0:4] = packed(growth)
    for k in range(1, 8):
        to = {"sp_0": wrap(z + k, 8)}
        wire.send(z_out, z_state.at[k], to, z_sem.at[0, k], when=z + k < 8)
        wire.send(z_dout, z_decay.at[k], to, z_sem.at[1, k], when=z + k < 8)
    gather[3]()
    within_block(2)
    within_block(3)
    z_acc[...] = jnp.zeros_like(z_acc)
    for k in range(7, 0, -1):

        @pl.when(z >= k)
        def _():
            src = {"sp_0": wrap(z - k, 8)}
            wire.arrive(z_state.at[k], z_sem.at[0, k], src)
            wire.arrive(z_decay.at[k], z_sem.at[1, k], src)
            z_acc[...] = z_acc[...] * unpacked(z_decay[k]) + z_state[k].astype(F32)

    begun = z_acc[...]
    for q in range(8):
        to_row[q] = (begun * row_dpre[q, 0:1] + row_pre[q]).astype(BF16)
    for k in range(1, 8):
        to = wrap(place + k, 8)
        wire.send(to_row.at[to], incoming.at[sixteen(place)], row_dev(to), back_sem.at[k])
    incoming[sixteen(place), :] = to_row[place]
    gather[4]()
    gather[5]()
    for k in range(1, 8):
        src = wrap(place - k, 8)
        wire.arrive(incoming.at[sixteen(src)], back_sem.at[k], row_dev(src))

    turns = [wrap(y + 2, 4), wrap(y + 1, 4), wrap(y - 1, 4), y]

    def reduce_rows(part, sent, far, got, sems, fill):
        upper, lower = pl.ds(0, 64), pl.ds(64, 64)
        part(0)
        wire.send(sent.at[0, upper], far.at[0], right, sems.at[0])
        wire.send(sent.at[0, lower], far.at[1], left, sems.at[1])
        part(1)
        wire.send(sent.at[1, lower], got.at[0, lower], right, sems.at[2])
        part(2)
        wire.send(sent.at[2, upper], got.at[1, upper], left, sems.at[3])
        fill(0)
        wire.arrive(far.at[0], sems.at[0], left)
        sent[1, 0:64] = (sent[1, 0:64].astype(F32) + far[0].astype(F32)).astype(BF16)
        wire.send(sent.at[1, upper], got.at[0, upper], right, sems.at[4])
        wire.arrive(far.at[1], sems.at[1], right)
        sent[2, 64:128] = (sent[2, 64:128].astype(F32) + far[1].astype(F32)).astype(BF16)
        wire.send(sent.at[2, lower], got.at[1, lower], left, sems.at[5])
        part(3)
        fill(1)
        wire.arrive(got.at[0, lower], sems.at[2], left)
        wire.arrive(got.at[1, upper], sems.at[3], right)
        wire.arrive(got.at[0, upper], sems.at[4], left)
        wire.arrive(got.at[1, lower], sems.at[5], right)
        return sent[3].astype(F32) + got[0].astype(F32) + got[1].astype(F32)

    def mix_part(k):
        t = turns[k]
        span = pl.ds(pl.multiple_of(t * BLOCK, BLOCK), BLOCK)
        begin = states[t] + incoming[...].astype(F32) * decays[t, 0:1]
        gated = yw[span, :] + ec[span, :] * dot(cs[span, :], begin.astype(BF16))
        gated = gated * silu(valve[span, :].astype(F32))
        gated = gated * lax.rsqrt(jnp.mean(gated * gated, axis=-1, keepdims=True) + EPSILON)
        y_norm = (gated * cluster[...]).astype(BF16)
        for j in range(4):
            lanes = slice(j * 512, (j + 1) * 512)
            mix_out[k, :, lanes] = dot(y_norm, w_mix[:, lanes]).astype(BF16)

    def mix_fill(stage):
        for event in (gather[6:8], gather[8:11])[stage]:
            event()

    mixer = reduce_rows(mix_part, mix_out, mix_far, mix_in, mix_sem, mix_fill)
    normed = layer_norm(ALPHA * resid[...].astype(F32) + mixer, scale_one[...]).astype(BF16)

    def chunk(t):
        return pl.ds(pl.multiple_of(16 + t * BLOCK, 16), BLOCK)

    def chunk_half(t, h):
        return pl.ds(pl.multiple_of(16 + t * BLOCK + h * 64, 16), 64)

    nall[chunk(y), :] = normed
    for h in range(2):
        for dev, half_of in ((right, h), (left, 1 - h)):
            v = nall.at[chunk_half(y, half_of)]
            wire.send(v, v, dev, all_sem.at[0 if dev is right else 1, half_of])
    for k in range(4):
        wire.send(
            nall.at[pl.ds(pl.multiple_of(y * BLOCK + BLOCK, 16), 16)],
            nall.at[pl.ds(0, 16)],
            rank_dev(after, k),
            all_sem.at[3, 0],
            when=jnp.logical_and(has_next, y == 3),
        )

    def project(span):
        rows = nall[span, :]

        def tile(j, carry):
            lanes = pl.ds(pl.multiple_of(j * 256, 256), 256)
            gu[span, lanes] = (
                dot(rows, wv[:, :, :, :, lanes].reshape(D, 256)).astype(BF16).astype(F32)
            )
            return carry

        lax.fori_loop(0, 11, tile, 0)

    far_t, right_t, left_t = turns[0], turns[1], turns[2]
    v = nall.at[chunk_half(left_t, 0)]
    wire.arrive(v, all_sem.at[0, 0], left)
    wire.send(v, v, right, all_sem.at[2, 0])
    v = nall.at[chunk_half(right_t, 1)]
    wire.arrive(v, all_sem.at[1, 1], right)
    wire.send(v, v, left, all_sem.at[2, 1])
    for event in gather[11:]:
        event()
    project(chunk(y))

    @pl.when(has_last)
    def _():
        wire.arrive(nall.at[pl.ds(0, 16)], all_sem.at[3, 0], rank_dev(before, 3))

    @pl.when(jnp.logical_not(has_last))
    def _():
        nall[0:16] = jnp.zeros((16, D), BF16)

    project(pl.ds(0, 16))
    wire.arrive(nall.at[chunk_half(left_t, 1)], all_sem.at[0, 1], left)
    project(chunk(left_t))
    wire.arrive(nall.at[chunk_half(right_t, 0)], all_sem.at[1, 0], right)
    project(chunk(right_t))
    wire.arrive(nall.at[chunk_half(far_t, 0)], all_sem.at[2, 0], left)
    wire.arrive(nall.at[chunk_half(far_t, 1)], all_sem.at[2, 1], right)
    project(chunk(far_t))

    def conv_gu(t, lanes, taps, tap_lanes):
        window = gu[pl.ds(pl.multiple_of(t * BLOCK + 8, 8), BLOCK + 8), lanes]
        weights = taps[:, tap_lanes].astype(F32)
        total = weights[0:1] * window[6 : 6 + BLOCK]
        for k in range(1, 3):
            total = total + weights[k : k + 1] * window[6 + k : 6 + k + BLOCK]
        return total

    def ffn_part(k):
        t = turns[k]
        pieces = []
        for j in range(11):
            lanes = slice(j * 128, (j + 1) * 128)
            shifted_lanes = slice(FF + j * 128, FF + (j + 1) * 128)
            gate = conv_gu(t, lanes, gate_taps, lanes)
            pieces.append((silu(gate) * conv_gu(t, shifted_lanes, up_taps, lanes)).astype(BF16))
        hidden = jnp.concatenate(pieces, axis=1)
        for j in range(4):
            w = wv[2 * j : 2 * j + 2, :, :, :, 2 * FF :].reshape(512, FF)
            ffn_out[k, :, j * 512 : (j + 1) * 512] = lax.dot_general(
                hidden, w, NT, preferred_element_type=F32
            ).astype(BF16)

    channel = reduce_rows(ffn_part, ffn_out, ffn_far, ffn_in, ffn_sem, lambda stage: None)
    out[...] = layer_norm(
        ALPHA * nall[chunk(y), :].astype(F32) + channel, scale_two[...]
    ).astype(BF16)
    wire.finish()


def shards(*arrays):
    arrays = [a.reshape(1, -1) if a.ndim == 1 else a for a in arrays]
    dma = pltpu.SemaphoreType.DMA
    scratch = [
        pltpu.VMEM((8, 4, 2, 32, COLS), BF16),
        pltpu.VMEM((16, INNER), BF16),
        pltpu.VMEM((16, STATE), BF16),
        pltpu.VMEM((16, STATE), BF16),
        pltpu.VMEM((ROWS, INNER), BF16),
        pltpu.VMEM((ROWS, STATE), BF16),
        pltpu.VMEM((ROWS, STATE), BF16),
        pltpu.VMEM((ROWS, 128), F32),
        pltpu.VMEM((BLOCKS, 2 * HEADS, BLOCK), F32),
        pltpu.VMEM((ROWS, INNER), F32),
        pltpu.VMEM((ROWS, INNER), F32),
        pltpu.VMEM((BLOCKS, STATE, INNER), F32),
        pltpu.VMEM((BLOCKS, 8, INNER), F32),
        pltpu.VMEM((STATE, INNER), BF16),
        pltpu.VMEM((8, 16, INNER), BF16),
        pltpu.VMEM((8, 8, 128), F32),
        pltpu.VMEM((8, 16, INNER), F32),
        pltpu.VMEM((8, 8, INNER), F32),
        pltpu.VMEM((8, 128), F32),
        pltpu.VMEM((8, 16, INNER), BF16),
        pltpu.VMEM((8, 8, 128), F32),
        pltpu.VMEM((16, INNER), BF16),
        pltpu.VMEM((8, 128), F32),
        pltpu.VMEM((16, INNER), F32),
        pltpu.VMEM((8, 16, INNER), BF16),
        pltpu.VMEM((STATE, INNER), BF16),
        pltpu.VMEM((4, BLOCK, D), BF16),
        pltpu.VMEM((2, 64, D), BF16),
        pltpu.VMEM((2, BLOCK, D), BF16),
        pltpu.VMEM((ROWS + 16, D), BF16),
        pltpu.VMEM((ROWS + 16, 2 * FF), F32),
        pltpu.VMEM((4, BLOCK, D), BF16),
        pltpu.VMEM((2, 64, D), BF16),
        pltpu.VMEM((2, BLOCK, D), BF16),
        dma((180,)),
        dma((54,)),
        dma,
        dma((3,)),
        dma((2, 8)),
        dma((2, 8)),
        dma((8,)),
        dma((6,)),
        dma((4, 2)),
        dma((6,)),
    ]
    return pl.pallas_call(
        layer_kernel,
        out_shape=jax.ShapeDtypeStruct((BLOCK, D), BF16),
        in_specs=[pl.BlockSpec(memory_space=pltpu.VMEM)] * len(arrays),
        out_specs=pl.BlockSpec(memory_space=pltpu.VMEM),
        scratch_shapes=scratch,
        compiler_params=pltpu.CompilerParams(
            collective_id=0, has_side_effects=True, vmem_limit_bytes=67043328
        ),
    )(*arrays)


def solution(mesh):
    split = Mesh(mesh.devices.reshape(8, 4, 2, mesh.shape["tp"]), ("sp_0", "sp_1", "sp_2", "tp"))
    in_specs = (
        P(SP_TP, None),
        P(SP, "tp"),
        P(SP, "tp"),
        P(SP, "tp"),
        P(SP, "tp"),
        P(SP, "tp"),
        P("tp"),
        P("tp"),
        P(SP, "tp"),
        P("tp"),
        P(None, "tp"),
        P(None, "tp"),
        P(None, "tp"),
        P("tp"),
        P("tp", None),
        P(),
        P(SP, "tp"),
        P(SP, "tp"),
        P("tp", SP),
        P(None, "tp"),
        P(None, "tp"),
        P(),
    )
    out_specs = P(SP_TP, None)
    return jax.shard_map(
        shards, mesh=split, in_specs=in_specs, out_specs=out_specs, check_vma=False
    )
```

time: 274 us -> 133 us (0.49)
  Pallas kernels: 0 us -> 126 us
  blocking collectives: 94 us -> 0 us
  waiting for transfers between devices: 73.7 us -> 0 us
  matrix products: 31.1 us -> 0 us
  other arithmetic: 25.9 us -> 0 us
  starting transfers between devices: 19.1 us -> 0 us
  between operations: 14 us -> 0.01 us
  local copies, waits for them, and re-layouts: 15.4 us -> 6.79 us
    pallas_call x0 -> x1, Pallas kernels: none -> 126 us  [shards(): pl.pallas_call(layer_kernel, out_shape=jax.ShapeDtypeStruct((BLOCK, D), B...]
    all_to_all x2 -> x0, blocking collectives: 55.6 us -> none  [sent_and_summed(): lax.all_to_all(in_blocks(shard, dim, count), axis, 0, 0, tiled=True)]
    all_gather x2 -> x0, waiting for transfers between devices: 53.3 us -> none  [the longest x1 44.6 us: gather_turned(): out, at, finished = (lax.all_gather(both, axis, axis=0, tiled=True), 0, [])]
    all_gather x5 -> x0, blocking collectives: 38.4 us -> none  [entering(): lax.all_gather(part.astype(kind), axis)]
    dot_general x9 -> x0, matrix products: 31.1 us -> none  [the longest x1 7.63 us: shards(): jnp.dot(hidden, down_whole, preferred_element_type=jnp.float32)]
    all_to_all x1 -> x0, waiting for transfers between devices: 19.8 us -> none  [sent_to_all(): return lax.all_to_all(copies, axis, split_axis=0, concat_axis=0, tiled=True)]
    ppermute x5 -> x0, starting transfers between devices: 14.5 us -> none  [shifted(): return lax.ppermute(shard, axis, pairs)]
    convert_element_type x18 -> x0, other arithmetic: 7.96 us -> none  [the longest x5 2.27 us: entering(): part.astype(kind)]
  transfers between devices with their start and end apart: 8 -> 0, of which waited for: 4 -> 0; matrix products, arithmetic and copies ran while one was open for 15% -> 0% of each run, Pallas kernels for 0% -> 0%
where the time goes in v1:
time: 133 us
  Pallas kernels  126 us (95%)
  local copies, waits for them, and re-layouts  6.79 us (5%)
    pallas_call x1, Pallas kernels, shards(): pl.pallas_call(layer_kernel, out_shape=jax.ShapeDtypeStruct((BLOCK, D), B...  126 us
    unnamed x4, local copies, waits for them, and re-layouts  6.79 us

profile of v1, /device:TPU:1, one launch (start us, length us, event | category | flops | bytes accessed | tf_op | source)
XLA Modules:
  0.0 133.2 jit_solution(10061605018115373630)
XLA Ops:
  0.0 1.6 %copy.23.deltas = f32[512,8]{1,0:T(8,128)} copy(f32[512,8]{0,1:T(8,128)} %param.27) | data formatting | bytes 32768 | tf_op args[5]
  1.6 1.6 %copy.24.fading = f32[512,8]{1,0:T(8,128)} copy(f32[512,8]{0,1:T(8,128)} %param.30) | data formatting | bytes 32768 | tf_op args[8]
  3.1 1.8 %copy.25.w_down = bf16[1408,32]{1,0:T(8,128)(2,1)} copy(bf16[1408,32]{0,1:T(8,128)(2,1)} %param.40) | data formatting | bytes 180224 | tf_op args[18]
  4.9 126.4 %shard_map.208 = bf16[128,2048]{1,0:T(8,128)(2,1)} custom-call(bf16[128,2048]{1,0:T(8,128)(2,1)} %resid.1, bf16[512,512]{1,0:T(8,128)(2,1)} %valve.1, bf16[512,512]{1,0:T(8,128)(2,1)} %x_in.1, bf16[512,128]{1,0:T(8,128)(2,1)} %b_in.1, bf16[512,128]{1,0:T(8,128)(2,1)} %c_in.1, f32[512,8]{1,0:T(8,128)} %copy.23.deltas, f32[1,8]{1,0:T(1,128)} %bitcast.9, ...), custom_call_target="tpu_custom_call" | custom-call | tf_op jit(solution)/shard_map/pallas_call | solution.py:696
  131.3 1.9 %copy.27 = bf16[128,2048]{1,0:T(8,128)(2,1)} copy(bf16[128,2048]{1,0:T(8,128)(2,1)} %shard_map.208) | data formatting | bytes 1048576

commit v2 on v1

--- a/solution.py
+++ b/solution.py
@@ -16,7 +16,7 @@
 D = 2048
 FF = 1408
 COLS = 3 * FF
-NA = 1664
+NA = 1792
 EPSILON = 1e-05
 ALPHA = 2.0**0.25
 SP = ("sp_0", "sp_1", "sp_2")
@@ -29,6 +29,21 @@
 
 def wrap(value, count):
     return lax.rem(value + 2 * count, count)
+
+
+class Marks:
+    def __init__(self):
+        self.scope = None
+
+    def __call__(self, name):
+        self.end()
+        self.scope = jax.named_scope(name)
+        self.scope.__enter__()
+
+    def end(self):
+        if self.scope is not None:
+            self.scope.__exit__(None, None, None)
+            self.scope = None
 
 
 class Wire:
@@ -71,7 +86,7 @@
                 pl.when(when)(copy.wait_send)
 
 
-def weight_gather(wire, wv, rsem, psem, ids):
+def weight_gather(wire, wv, rsem, psem, ids, mark):
     z, x, c, _ = ids
     cols_a, cols_b = pl.ds(0, NA), pl.ds(NA, COLS - NA)
     half, whole = (pl.ds(0, 16), pl.ds(16, 16)), pl.ds(0, 32)
@@ -80,6 +95,9 @@
     other = {"sp_2": 1 - c}
     xl, xr, xf = wrap(x - 1, 4), wrap(x + 1, 4), wrap(x + 2, 4)
 
+    def pair(off):
+        return psem.at[off % 8]
+
     def piece(zz, xx, cols, rows=whole):
         return wv.at[zz, xx, c, rows, cols]
 
@@ -98,9 +116,6 @@
     def a1f(d):
         return rsem.at[4 + d]
 
-    def a2(d, s):
-        return rsem.at[6 + d * 4 + s - 1]
-
     def b1(d, s):
         return rsem.at[14 + d * 4 + s - 1]
 
@@ -110,20 +125,26 @@
     def b2f(d, s):
         return rsem.at[38 + d * 8 + s]
 
-    def along_x(off):
+    def a2(d, s, k):
+        return rsem.at[54 + d * 16 + (s - 1) * 4 + k]
+
+    columns = (x, xl, xr, xf)
+
+    def x_send(off):
         v = piece(wrap(z + off, 8), x, cols_b)
         send(v, xp, b2(0, off % 8))
         send(v, xm, b2(1, off % 8))
-        send(v, other, psem)
 
     def start():
-        send(piece(z, x, cols_b), zp, b1(0, 1))
-        send(piece(z, x, cols_b), zm, b1(1, 1))
         send(piece(z, x, cols_a, half[0]), xp, a1(0, 0))
         send(piece(z, x, cols_a, half[1]), xm, a1(1, 1))
         send(piece(z, x, cols_a, half[1]), xp, a1(0, 1))
         send(piece(z, x, cols_a, half[0]), xm, a1(1, 0))
-        along_x(0)
+        send(piece(z, x, cols_b), zp, b1(0, 1))
+        send(piece(z, x, cols_b), zm, b1(1, 1))
+        send(piece(z, x, cols_a), zp, a2(0, 1, 0))
+        send(piece(z, x, cols_a), zm, a2(1, 1, 0))
+        send(piece(z, x, cols_b), other, pair(0))
 
     def row_far():
         v = piece(z, xl, cols_a, half[0])
@@ -138,9 +159,10 @@
         arrive(piece(z, xr, cols_a, half[0]), a1(1, 0))
         arrive(piece(z, xf, cols_a, half[0]), a1f(0))
         arrive(piece(z, xf, cols_a, half[1]), a1f(1))
-        send(group(z), zp, a2(0, 1))
-        send(group(z), zm, a2(1, 1))
-        send(group(z), other, psem)
+        for k in range(1, 4):
+            send(piece(z, columns[k], cols_a), zp, a2(0, 1, k))
+            send(piece(z, columns[k], cols_a), zm, a2(1, 1, k))
+        send(group(z), other, pair(0))
 
     def z_piece(s):
         zl, zr = wrap(z - s, 8), wrap(z + s, 8)
@@ -148,70 +170,72 @@
             v = piece(zl, x, cols_b)
             arrive(v, b1(0, s))
             send(v if s < 3 else piece(zl, x, cols_b, half[0]), zp, b1(0, s + 1))
+            send(v, other, pair(-s))
             v = piece(zr, x, cols_b)
             arrive(v, b1(1, s))
             send(v if s < 3 else piece(zr, x, cols_b, half[1]), zm, b1(1, s + 1))
-            along_x(-s)
-            along_x(s)
+            send(v, other, pair(s))
         else:
             arrive(piece(zl, x, cols_b, half[0]), b1(0, 4))
             arrive(piece(zl, x, cols_b, half[1]), b1(1, 4))
-            along_x(4)
-
-    def z_group(s):
+            send(piece(zl, x, cols_b), other, pair(4))
+
+    def z_group(s, *which):
         zl, zr = wrap(z - s, 8), wrap(z + s, 8)
-        if s < 4:
-            arrive(group(zl), a2(0, s))
-            send(group(zl) if s < 3 else group(zl, half[0]), zp, a2(0, s + 1))
-            arrive(group(zr), a2(1, s))
-            send(group(zr) if s < 3 else group(zr, half[1]), zm, a2(1, s + 1))
-            send(group(zl), other, psem)
-            send(group(zr), other, psem)
-        else:
-            arrive(group(zl, half[0]), a2(0, 4))
-            arrive(group(zl, half[1]), a2(1, 4))
-            send(group(zl), other, psem)
+        for k in which:
+            if s < 4:
+                v = piece(zl, columns[k], cols_a)
+                arrive(v, a2(0, s, k))
+                send(v if s < 3 else piece(zl, columns[k], cols_a, half[0]), zp, a2(0, s + 1, k))
+                v = piece(zr, columns[k], cols_a)
+                arrive(v, a2(1, s, k))
+                send(v if s < 3 else piece(zr, columns[k], cols_a, half[1]), zm, a2(1, s + 1, k))
+            else:
+                arrive(piece(zl, columns[k], cols_a, half[0]), a2(0, 4, k))
+                arrive(piece(zl, columns[k], cols_a, half[1]), a2(1, 4, k))
+        if 3 in which:
+            send(group(zl), other, pair(-s))
+            if s < 4:
+                send(group(zr), other, pair(s))
 
     def x_piece(off):
         zz = wrap(z + off, 8)
         v = piece(zz, xl, cols_b)
         arrive(v, b2(0, off % 8))
         send(piece(zz, xl, cols_b, half[0]), xp, b2f(0, off % 8))
-        send(v, other, psem)
+        send(v, other, pair(off))
         v = piece(zz, xr, cols_b)
         arrive(v, b2(1, off % 8))
         send(piece(zz, xr, cols_b, half[1]), xm, b2f(1, off % 8))
-        send(v, other, psem)
+        send(v, other, pair(off))
 
     def x_far(off):
         zz = wrap(z + off, 8)
         arrive(piece(zz, xf, cols_b, half[0]), b2f(0, off % 8))
         arrive(piece(zz, xf, cols_b, half[1]), b2f(1, off % 8))
-        send(piece(zz, xf, cols_b), other, psem)
-
-    def finish():
-        arrive(wv.at[pl.ds(0, 4)], psem)
-
-    return [
-        start,
-        row_far,
-        lambda: z_piece(1),
-        row_done,
-        lambda: x_piece(0),
-        lambda: z_piece(2),
-        lambda: (x_piece(-1), x_piece(1)),
-        lambda: z_group(1),
-        lambda: z_piece(3),
-        lambda: (x_piece(-2), x_piece(2), x_far(0)),
-        lambda: z_piece(4),
-        lambda: z_group(2),
-        lambda: (x_piece(-3), x_piece(3), x_far(1), x_far(-1)),
-        lambda: (x_piece(4), x_far(2), x_far(-2)),
-        lambda: z_group(3),
-        lambda: (x_far(3), x_far(-3), x_far(4)),
-        lambda: z_group(4),
-        finish,
-    ]
+        send(piece(zz, xf, cols_b), other, pair(off))
+
+    def pair_done(off):
+        arrive(wv.at[wrap(z + off, 8), :, 1 - c], pair(off))
+
+    steps = {
+        "start": start,
+        "row_far": row_far,
+        "row_done": row_done,
+        "z_piece": z_piece,
+        "z_group": z_group,
+        "x_send": x_send,
+        "x_piece": x_piece,
+        "x_far": x_far,
+        "pair_done": pair_done,
+    }
+
+    def run(*plan):
+        for name, *at in plan:
+            mark("g_" + name + "".join(str(k) for k in at))
+            steps[name](*at)
+
+    return run
 
 
 def thirds(v):
@@ -225,10 +249,6 @@
     return jnp.dot(a, b, preferred_element_type=F32)
 
 
-def exact_left(selector, v):
-    return sum(dot(selector, part) for part in thirds(v))
-
-
 def spread(v, onehot):
     return sum(dot(part, onehot) for part in thirds(v))
 
@@ -243,75 +263,103 @@
     return centred * lax.rsqrt(spread_of + EPSILON) * scales
 
 
-def layer_kernel(
-    resid,
-    valve,
-    x_in,
-    b_in,
-    c_in,
-    deltas,
-    offset,
-    speed,
-    fading,
-    bypass,
-    x_taps,
-    b_taps,
-    c_taps,
-    cluster,
-    w_mix,
-    scale_one,
-    w_gate,
-    w_up,
-    w_down,
-    gate_taps,
-    up_taps,
-    scale_two,
-    out,
-    wv,
-    x_rim,
-    b_rim,
-    c_rim,
-    xs,
-    bs,
-    cs,
-    cums,
-    turned,
-    ec,
-    yw,
-    states,
-    decays,
-    ends,
-    row_ends,
-    row_decay,
-    row_pre,
-    row_dpre,
-    own_decay,
-    z_state,
-    z_decay,
-    z_out,
-    z_dout,
-    z_acc,
-    to_row,
-    incoming,
-    mix_out,
-    mix_far,
-    mix_in,
-    nall,
-    gu,
-    ffn_out,
-    ffn_far,
-    ffn_in,
-    send_sem,
-    gather_sem,
-    pair_sem,
-    rim_sem,
-    row_sem,
-    z_sem,
-    back_sem,
-    mix_sem,
-    all_sem,
-    ffn_sem,
-):
+LOADED = (
+    "resid",
+    "valve",
+    "x_in",
+    "b_in",
+    "c_in",
+    "deltas",
+    "offset",
+    "speed",
+    "fading",
+    "bypass",
+    "x_taps",
+    "b_taps",
+    "c_taps",
+    "cluster",
+    "w_mix",
+    "scale_one",
+    "gate_taps",
+    "up_taps",
+    "scale_two",
+)
+
+
+EARLY = LOADED[2:13]
+
+
+def layer_kernel(*refs):
+    sources, out, refs = refs[:22], refs[22], refs[23:]
+    loads, refs = refs[:19], refs[19:]
+    (
+        resid,
+        valve,
+        x_in,
+        b_in,
+        c_in,
+        deltas,
+        offset,
+        speed,
+        fading,
+        bypass,
+        x_taps,
+        b_taps,
+        c_taps,
+        cluster,
+        w_mix,
+        scale_one,
+        gate_taps,
+        up_taps,
+        scale_two,
+    ) = loads
+    (
+        wv,
+        load_sem,
+        x_rim,
+        b_rim,
+        c_rim,
+        xs,
+        bs,
+        cs,
+        cums,
+        turned,
+        ec,
+        yw,
+        states,
+        decays,
+        ends,
+        row_ends,
+        row_decay,
+        row_pre,
+        row_dpre,
+        own_decay,
+        z_state,
+        z_decay,
+        z_out,
+        z_dout,
+        z_acc,
+        to_row,
+        incoming,
+        mix_out,
+        mix_far,
+        mix_in,
+        nall,
+        gu,
+        ffn_out,
+        ffn_far,
+        ffn_in,
+        send_sem,
+        gather_sem,
+        pair_sem,
+        rim_sem,
+        row_sem,
+        z_sem,
+        back_sem,
+        mix_sem,
+        all_sem,
+        ffn_sem,
+    ) = refs
     ids = tuple(lax.axis_index(name) for name in SP_TP)
     z, x, c, y = ids
     rank = z * 8 + x * 2 + c
@@ -330,6 +378,8 @@
     after, before = wrap(rank + 1, 64), wrap(rank - 1, 64)
     right, left = {"tp": wrap(y + 1, 4)}, {"tp": wrap(y - 1, 4)}
 
+    mark = Marks()
+    mark("barrier")
     sem = pltpu.get_barrier_semaphore()
     greeted = [{"sp_0": wrap(z + k, 8)} for k in range(1, 8)]
     greeted += [row_dev(wrap(place + k, 8)) for k in range(1, 8)]
@@ -338,31 +388,44 @@
     for dev in greeted:
         pl.semaphore_signal(sem, inc=1, device_id=dev, device_id_type=MESH)
 
-    ident = (
-        lax.broadcasted_iota(jnp.int32, (32, 32), 0) == lax.broadcasted_iota(jnp.int32, (32, 32), 1)
-    ).astype(BF16)
-    wv[z, x, c, :, 0:FF] = w_gate[...]
-    wv[z, x, c, :, FF : 2 * FF] = w_up[...]
-    wv[z, x, c, :, 2 * FF :] = lax.dot_general(
-        ident, w_down[...], NT, preferred_element_type=F32
-    ).astype(BF16)
+    sources, shards_here = sources[:16] + sources[19:], sources[16:19]
+    copies = [
+        pltpu.make_async_copy(src, wv.at[z, x, c, :, pl.ds(k * FF, FF)], load_sem.at[19 + k])
+        for k, src in enumerate(shards_here)
+    ]
+    order = sorted(range(19), key=lambda k: LOADED[k] not in EARLY)
+    copies += [pltpu.make_async_copy(sources[k], loads[k], load_sem.at[k]) for k in order]
+    for copy in copies:
+        copy.start()
+    for copy in copies[: 3 + len(EARLY)]:
+        copy.wait()
     pl.semaphore_wait(sem, len(greeted))
 
     has_next, has_last = rank < 63, rank > 0
     last = pl.ds(ROWS - 16, 16)
     for k, (src, dst) in enumerate(((x_in, x_rim), (b_in, b_rim), (c_in, c_rim))):
         wire.send(src.at[last], dst, rank_dev(after), rim_sem.at[k], when=has_next)
-    gather = weight_gather(wire, wv, gather_sem, pair_sem, ids)
-    gather[0]()
+    gather = weight_gather(wire, wv, gather_sem, pair_sem, ids, mark)
+    gather(("start",))
 
     rows_at = lax.broadcasted_iota(jnp.int32, (BLOCK, BLOCK), 0)
     cols_at = lax.broadcasted_iota(jnp.int32, (BLOCK, BLOCK), 1)
     causal = rows_at >= cols_at
-    tril = causal.astype(BF16)
+    triu = (rows_at <= cols_at).astype(BF16)
     onehot = (
         lax.broadcasted_iota(jnp.int32, (HEADS, INNER), 0)
         == lax.div(lax.broadcasted_iota(jnp.int32, (HEADS, INNER), 1), HEAD_DIM)
     ).astype(BF16)
+    eye = lax.broadcasted_iota(jnp.int32, (HEADS, HEADS), 0) == lax.broadcasted_iota(
+        jnp.int32, (HEADS, HEADS), 1
+    )
+
+    def turned_up(v):
+        return jnp.sum(
+            jnp.where(eye, jnp.broadcast_to(v[...], (HEADS, HEADS)), 0.0), axis=1, keepdims=True
+        )
+
+    offset_col, speed_col = turned_up(offset), turned_up(speed)
     skip = spread(jnp.broadcast_to(bypass[...], (8, HEADS)), onehot)[0:1]
     low_lanes = lax.broadcasted_iota(jnp.int32, (BLOCK, 2 * HEAD_DIM), 1) < HEAD_DIM
 
@@ -384,12 +447,14 @@
         xs[span] = x_act
         bs[span] = b_act
         cs[span] = conv_block(c_in, c_rim, c_taps, b).astype(BF16)
-        raw = deltas[span] + offset[...]
-        step = jnp.maximum(raw, 0.0) + jnp.log1p(jnp.exp(-jnp.abs(raw)))
-        cum = exact_left(tril, fading[span] - speed[...] * step)
-        cums[span, 0:HEADS] = cum
-        cums[span, HEADS : 2 * HEADS] = step
-        turned[b] = cums[span].T[0 : 2 * HEADS]
+        raw = deltas[:, span] + offset_col
+        step_rows = jnp.maximum(raw, 0.0) + jnp.log1p(jnp.exp(-jnp.abs(raw)))
+        cum_rows = spread(fading[:, span] - speed_col * step_rows, triu)
+        both = jnp.concatenate([cum_rows, step_rows], axis=0)
+        turned[b] = both
+        both = jnp.concatenate([both, jnp.zeros((112, BLOCK), F32)], axis=0).T
+        cums[span] = both
+        cum, step = both[:, 0:HEADS], both[:, HEADS : 2 * HEADS]
         grown = spread(jnp.exp(cum), onehot)
         ec[span] = grown
         to_end = spread(step * jnp.exp(cum[BLOCK - 1 : BLOCK] - cum), onehot)
@@ -422,11 +487,13 @@
     def unpacked(tile):
         return jnp.concatenate([tile[k : k + 1] for k in range(4)], axis=1)
 
-    cums[...] = jnp.zeros_like(cums)
+    mark("local3")
     local_block(3)
-    gather[1]()
+    mark("local2")
     local_block(2)
     local_block(1)
+    gather(("row_far",))
+    mark("rim_wait")
 
     @pl.when(has_last)
     def _():
@@ -438,7 +505,9 @@
         for dst in (x_rim, b_rim, c_rim):
             dst[...] = jnp.zeros_like(dst)
 
+    mark("local0")
     local_block(0)
+    mark("ends")
 
     total = jnp.zeros((STATE, INNER), F32)
     growth = jnp.ones((1, INNER), F32)
@@ -449,8 +518,7 @@
         total = total * decay + fresh
         growth = growth * decay
     ends[...] = total.astype(BF16)
-    own_decay[...] = jnp.zeros_like(own_decay)
-    own_decay[0:4] = packed(growth)
+    own_decay[...] = packed(growth)
 
     def sixteen(p):
         return pl.ds(pl.multiple_of(p * 16, 16), 16)
@@ -461,13 +529,16 @@
         wire.send(own_decay, row_decay.at[place], row_dev(to), row_sem.at[1, k])
     row_ends[place] = ends[sixteen(place), :]
     row_decay[place] = own_decay[...]
-    gather[2]()
+    gather(("x_send", 0), ("z_piece", 1))
+    mark("within01")
     within_block(0)
     within_block(1)
+    mark("row_wait")
     for k in range(1, 8):
         src = wrap(place - k, 8)
         wire.arrive(row_ends.at[src], row_sem.at[0, k], row_dev(src))
         wire.arrive(row_decay.at[src], row_sem.at[1, k], row_dev(src))
+    mark("row_fold")
     total = jnp.zeros((16, INNER), F32)
     growth = jnp.ones((1, INNER), F32)
     for q in range(8):
@@ -477,15 +548,16 @@
         total = total * decay + row_ends[q].astype(F32)
         growth = growth * decay
     z_out[...] = total.astype(BF16)
-    z_dout[...] = jnp.zeros_like(z_dout)
-    z_dout[0:4] = packed(growth)
+    z_dout[...] = packed(growth)
     for k in range(1, 8):
         to = {"sp_0": wrap(z + k, 8)}
         wire.send(z_out, z_state.at[k], to, z_sem.at[0, k], when=z + k < 8)
         wire.send(z_dout, z_decay.at[k], to, z_sem.at[1, k], when=z + k < 8)
-    gather[3]()
+    gather(("row_done",))
+    mark("within23")
     within_block(2)
     within_block(3)
+    mark("z_wait")
     z_acc[...] = jnp.zeros_like(z_acc)
     for k in range(7, 0, -1):
 
@@ -496,6 +568,7 @@
             wire.arrive(z_decay.at[k], z_sem.at[1, k], src)
             z_acc[...] = z_acc[...] * unpacked(z_decay[k]) + z_state[k].astype(F32)
 
+    mark("z_fold")
     begun = z_acc[...]
     for q in range(8):
         to_row[q] = (begun * row_dpre[q, 0:1] + row_pre[q]).astype(BF16)
@@ -503,36 +576,61 @@
         to = wrap(place + k, 8)
         wire.send(to_row.at[to], incoming.at[sixteen(place)], row_dev(to), back_sem.at[k])
     incoming[sixteen(place), :] = to_row[place]
-    gather[4]()
-    gather[5]()
+    gather(("x_send", -1), ("x_send", 1), ("x_piece", 0), ("z_piece", 2))
+    mark("back_wait")
     for k in range(1, 8):
         src = wrap(place - k, 8)
         wire.arrive(incoming.at[sixteen(src)], back_sem.at[k], row_dev(src))
 
+    for copy in copies[3 + len(EARLY) :]:
+        copy.wait()
     turns = [wrap(y + 2, 4), wrap(y + 1, 4), wrap(y - 1, 4), y]
 
-    def reduce_rows(part, sent, far, got, sems, fill):
+    def reduce_rows(part, sent, far, got, sems, fill, name):
         upper, lower = pl.ds(0, 64), pl.ds(64, 64)
-        part(0)
-        wire.send(sent.at[0, upper], far.at[0], right, sems.at[0])
-        wire.send(sent.at[0, lower], far.at[1], left, sems.at[1])
-        part(1)
-        wire.send(sent.at[1, lower], got.at[0, lower], right, sems.at[2])
-        part(2)
-        wire.send(sent.at[2, upper], got.at[1, upper], left, sems.at[3])
+        tiles = [pl.ds(j * 512, 512) for j in range(4)]
+        mark(name + "_part0")
+        tile = part(0)
+        for j, lanes in enumerate(tiles):
+            tile(j)
+            wire.send(sent.at[0, upper, lanes], far.at[0, :, lanes], right, sems.at[j])
+            wire.send(sent.at[0, lower, lanes], far.at[1, :, lanes], left, sems.at[4 + j])
+        mark(name + "_part1")
+        tile = part(1)
+        for j in range(4):
+            tile(j)
+        wire.send(sent.at[1, lower], got.at[0, lower], right, sems.at[8])
+        mark(name + "_part2")
+        tile = part(2)
+        for j in range(4):
+            tile(j)
+        wire.send(sent.at[2, upper], got.at[1, upper], left, sems.at[9])
         fill(0)
-        wire.arrive(far.at[0], sems.at[0], left)
-        sent[1, 0:64] = (sent[1, 0:64].astype(F32) + far[0].astype(F32)).astype(BF16)
-        wire.send(sent.at[1, upper], got.at[0, upper], right, sems.at[4])
-        wire.arrive(far.at[1], sems.at[1], right)
-        sent[2, 64:128] = (sent[2, 64:128].astype(F32) + far[1].astype(F32)).astype(BF16)
-        wire.send(sent.at[2, lower], got.at[1, lower], left, sems.at[5])
-        part(3)
+        mark(name + "_far_wait")
+        for j, lanes in enumerate(tiles):
+            at = slice(j * 512, (j + 1) * 512)
+            wire.arrive(far.at[0, :, lanes], sems.at[j], left)
+            sent[1, 0:64, at] = (sent[1, 0:64, at].astype(F32) + far[0, :, at].astype(F32)).astype(
+                BF16
+            )
+            wire.send(sent.at[1, upper, lanes], got.at[0, upper, lanes], right, sems.at[10 + j])
+            wire.arrive(far.at[1, :, lanes], sems.at[4 + j], right)
+            sent[2, 64:, at] = (sent[2, 64:, at].astype(F32) + far[1, :, at].astype(F32)).astype(
+                BF16
+            )
+            wire.send(sent.at[2, lower, lanes], got.at[1, lower, lanes], left, sems.at[14 + j])
         fill(1)
-        wire.arrive(got.at[0, lower], sems.at[2], left)
-        wire.arrive(got.at[1, upper], sems.at[3], right)
-        wire.arrive(got.at[0, upper], sems.at[4], left)
-        wire.arrive(got.at[1, lower], sems.at[5], right)
+        mark(name + "_part3")
+        tile = part(3)
+        for j in range(4):
+            tile(j)
+        fill(2)
+        mark(name + "_wait")
+        wire.arrive(got.at[0, lower], sems.at[8], left)
+        wire.arrive(got.at[1, upper], sems.at[9], right)
+        for j, lanes in enumerate(tiles):
+            wire.arrive(got.at[0, upper, lanes], sems.at[10 + j], left)
+            wire.arrive(got.at[1, lower, lanes], sems.at[14 + j], right)
         return sent[3].astype(F32) + got[0].astype(F32) + got[1].astype(F32)
 
     def mix_part(k):
@@ -543,15 +641,24 @@
         gated = gated * silu(valve[span, :].astype(F32))
         gated = gated * lax.rsqrt(jnp.mean(gated * gated, axis=-1, keepdims=True) + EPSILON)
         y_norm = (gated * cluster[...]).astype(BF16)
-        for j in range(4):
+
+        def tile(j):
             lanes = slice(j * 512, (j + 1) * 512)
             mix_out[k, :, lanes] = dot(y_norm, w_mix[:, lanes]).astype(BF16)
 
+        return tile
+
     def mix_fill(stage):
-        for event in (gather[6:8], gather[8:11])[stage]:
-            event()
-
-    mixer = reduce_rows(mix_part, mix_out, mix_far, mix_in, mix_sem, mix_fill)
+        if stage == 0:
+            gather(("x_send", -2), ("x_send", 2), ("z_group", 1, 0, 1), ("x_piece", -1), ("z_group", 1, 2, 3))
+        elif stage == 1:
+            gather(("z_piece", 3), ("x_piece", 1), ("x_send", -3), ("x_send", 3))
+        else:
+            gather(("x_piece", -2), ("x_piece", 2), ("x_far", 0))
+            gather(("z_group", 2, 0, 1), ("z_piece", 4), ("z_group", 2, 2, 3), ("x_send", 4), ("x_far", -1), ("x_far", 1))
+
+    mixer = reduce_rows(mix_part, mix_out, mix_far, mix_in, mix_sem, mix_fill, "mix")
+    mark("norm_one")
     normed = layer_norm(ALPHA * resid[...].astype(F32) + mixer, scale_one[...]).astype(BF16)
 
     def chunk(t):
@@ -561,6 +668,7 @@
         return pl.ds(pl.multiple_of(16 + t * BLOCK + h * 64, 16), 64)
 
     nall[chunk(y), :] = normed
+    mark("all_send")
     for h in range(2):
         for dev, half_of in ((right, h), (left, 1 - h)):
             v = nall.at[chunk_half(y, half_of)]
@@ -574,28 +682,58 @@
             when=jnp.logical_and(has_next, y == 3),
         )
 
-    def project(span):
-        rows = nall[span, :]
-
-        def tile(j, carry):
-            lanes = pl.ds(pl.multiple_of(j * 256, 256), 256)
-            gu[span, lanes] = (
-                dot(rows, wv[:, :, :, :, lanes].reshape(D, 256)).astype(BF16).astype(F32)
-            )
-            return carry
-
-        lax.fori_loop(0, 11, tile, 0)
+    def project(spans, offs, first, last_of):
+        zs = [wrap(z + off, 8) for off in offs]
+        deep = [pl.ds(pl.multiple_of(zz * 256, 256), 256) for zz in zs]
+        rows = jnp.concatenate(
+            [jnp.concatenate([nall[span, k] for k in deep], axis=1) for span in spans], axis=0
+        )
+
+        for j in range(11):
+            lanes = slice(j * 256, (j + 1) * 256)
+            weights = [wv[zz, :, :, :, lanes].reshape(256, 256) for zz in zs]
+            got = dot(rows, jnp.concatenate(weights, axis=0))
+            at = 0
+            for span in spans:
+                mine = got[at : at + span.size]
+                at += span.size
+                if not first:
+                    mine = mine + gu[span, lanes]
+                gu[span, lanes] = mine.astype(BF16).astype(F32) if last_of else mine
 
     far_t, right_t, left_t = turns[0], turns[1], turns[2]
+    whole, inner, outer = range(8), (0, 1, -1), (2, -2)
+    rest = (3, -3, 4)
+    gather(("x_piece", -3), ("pair_done", 0), ("pair_done", 1), ("pair_done", -1))
+    own = (chunk(y),)
+    mark("project_own")
+    project(own, inner, True, False)
+    gather(("x_piece", 3), ("x_far", -2), ("x_far", 2), ("z_group", 3, 0, 1, 2, 3))
+    gather(("x_piece", 4))
+    mark("all_first")
     v = nall.at[chunk_half(left_t, 0)]
     wire.arrive(v, all_sem.at[0, 0], left)
     wire.send(v, v, right, all_sem.at[2, 0])
     v = nall.at[chunk_half(right_t, 1)]
     wire.arrive(v, all_sem.at[1, 1], right)
     wire.send(v, v, left, all_sem.at[2, 1])
-    for event in gather[11:]:
-        event()
-    project(chunk(y))
+    gather(("x_far", -3), ("x_far", 3), ("pair_done", 2), ("pair_done", -2))
+    mark("project_own2")
+    project(own, outer, False, False)
+    gather(("x_far", 4),)
+    mark("near_wait")
+    wire.arrive(nall.at[chunk_half(left_t, 1)], all_sem.at[0, 1], left)
+    wire.arrive(nall.at[chunk_half(right_t, 0)], all_sem.at[1, 0], right)
+    near = (chunk(left_t), chunk(right_t))
+    mark("project_near")
+    project(near, inner + outer, True, False)
+    gather(("z_group", 4, 0, 1, 2, 3), ("pair_done", 3), ("pair_done", -3), ("pair_done", 4))
+    mark("project_rest")
+    project(own + near, rest, False, True)
+    mark("far_wait")
+    wire.arrive(nall.at[chunk_half(far_t, 0)], all_sem.at[2, 0], left)
+    wire.arrive(nall.at[chunk_half(far_t, 1)], all_sem.at[2, 1], right)
+    mark("halo")
 
     @pl.when(has_last)
     def _():
@@ -604,15 +742,8 @@
     @pl.when(jnp.logical_not(has_last))
     def _():
         nall[0:16] = jnp.zeros((16, D), BF16)
-
-    project(pl.ds(0, 16))
-    wire.arrive(nall.at[chunk_half(left_t, 1)], all_sem.at[0, 1], left)
-    project(chunk(left_t))
-    wire.arrive(nall.at[chunk_half(right_t, 0)], all_sem.at[1, 0], right)
-    project(chunk(right_t))
-    wire.arrive(nall.at[chunk_half(far_t, 0)], all_sem.at[2, 0], left)
-    wire.arrive(nall.at[chunk_half(far_t, 1)], all_sem.at[2, 1], right)
-    project(chunk(far_t))
+    mark("project_far")
+    project((chunk(far_t), pl.ds(0, 16)), whole, True, True)
 
     def conv_gu(t, lanes, taps, tap_lanes):
         window = gu[pl.ds(pl.multiple_of(t * BLOCK + 8, 8), BLOCK + 8), lanes]
@@ -631,24 +762,34 @@
             gate = conv_gu(t, lanes, gate_taps, lanes)
             pieces.append((silu(gate) * conv_gu(t, shifted_lanes, up_taps, lanes)).astype(BF16))
         hidden = jnp.concatenate(pieces, axis=1)
-        for j in range(4):
+
+        def tile(j):
             w = wv[2 * j : 2 * j + 2, :, :, :, 2 * FF :].reshape(512, FF)
             ffn_out[k, :, j * 512 : (j + 1) * 512] = lax.dot_general(
                 hidden, w, NT, preferred_element_type=F32
             ).astype(BF16)
 
-    channel = reduce_rows(ffn_part, ffn_out, ffn_far, ffn_in, ffn_sem, lambda stage: None)
+        return tile
+
+    channel = reduce_rows(ffn_part, ffn_out, ffn_far, ffn_in, ffn_sem, lambda stage: None, "ffn")
+    mark("norm_two")
     out[...] = layer_norm(
         ALPHA * nall[chunk(y), :].astype(F32) + channel, scale_two[...]
     ).astype(BF16)
+    mark("finish")
     wire.finish()
+    mark.end()
 
 
 def shards(*arrays):
     arrays = [a.reshape(1, -1) if a.ndim == 1 else a for a in arrays]
+    for k in (5, 8, 18):
+        arrays[k] = arrays[k].T
     dma = pltpu.SemaphoreType.DMA
-    scratch = [
+    loaded = arrays[:16] + arrays[19:]
+    scratch = [pltpu.VMEM(a.shape, a.dtype) for a in loaded] + [
         pltpu.VMEM((8, 4, 2, 32, COLS), BF16),
+        dma((22,)),
         pltpu.VMEM((16, INNER), BF16),
         pltpu.VMEM((16, STATE), BF16),
         pltpu.VMEM((16, STATE), BF16),
@@ -663,14 +804,14 @@
         pltpu.VMEM((BLOCKS, 8, INNER), F32),
         pltpu.VMEM((STATE, INNER), BF16),
         pltpu.VMEM((8, 16, INNER), BF16),
-        pltpu.VMEM((8, 8, 128), F32),
+        pltpu.VMEM((8, 4, 128), F32),
         pltpu.VMEM((8, 16, INNER), F32),
         pltpu.VMEM((8, 8, INNER), F32),
-        pltpu.VMEM((8, 128), F32),
+        pltpu.VMEM((4, 128), F32),
         pltpu.VMEM((8, 16, INNER), BF16),
-        pltpu.VMEM((8, 8, 128), F32),
+        pltpu.VMEM((8, 4, 128), F32),
         pltpu.VMEM((16, INNER), BF16),
-        pltpu.VMEM((8, 128), F32),
+        pltpu.VMEM((4, 128), F32),
         pltpu.VMEM((16, INNER), F32),
         pltpu.VMEM((8, 16, INNER), BF16),
         pltpu.VMEM((STATE, INNER), BF16),
@@ -682,21 +823,21 @@
         pltpu.VMEM((4, BLOCK, D), BF16),
         pltpu.VMEM((2, 64, D), BF16),
         pltpu.VMEM((2, BLOCK, D), BF16),
-        dma((180,)),
-        dma((54,)),
-        dma,
+        dma((260,)),
+        dma((86,)),
+        dma((8,)),
         dma((3,)),
         dma((2, 8)),
         dma((2, 8)),
         dma((8,)),
-        dma((6,)),
+        dma((18,)),
         dma((4, 2)),
-        dma((6,)),
+        dma((18,)),
     ]
     return pl.pallas_call(
         layer_kernel,
         out_shape=jax.ShapeDtypeStruct((BLOCK, D), BF16),
-        in_specs=[pl.BlockSpec(memory_space=pltpu.VMEM)] * len(arrays),
+        in_specs=[pl.BlockSpec(memory_space=pltpu.HBM)] * len(arrays),
         out_specs=pl.BlockSpec(memory_space=pltpu.VMEM),
         scratch_shapes=scratch,
         compiler_params=pltpu.CompilerParams(

time: 133 us -> 100 us (0.75)
  Pallas kernels: 126 us -> 98.5 us
  local copies, waits for them, and re-layouts: 6.79 us -> 1.88 us
    pallas_call x1, Pallas kernels: 126 us -> 98.5 us  [shards(): pl.pallas_call(layer_kernel, out_shape=jax.ShapeDtypeStruct((BLOCK, D), B...]
    unnamed x4 -> x1, local copies, waits for them, and re-layouts: 6.79 us -> 1.88 us
where the time goes in v2:
time: 100 us
  Pallas kernels  98.5 us (98%)
  local copies, waits for them, and re-layouts  1.88 us (2%)
    pallas_call x1, Pallas kernels, shards(): pl.pallas_call(layer_kernel, out_shape=jax.ShapeDtypeStruct((BLOCK, D), B...  98.5 us

profile of v2, /device:TPU:1, one launch (start us, length us, event | category | flops | bytes accessed | tf_op | source)
XLA Modules:
  0.0 100.3 jit_solution(4667890119515429889)
XLA Ops:
  0.0 98.5 %shard_map.208 = bf16[128,2048]{1,0:T(8,128)(2,1)} custom-call(bf16[128,2048]{1,0:T(8,128)(2,1)} %refs_0_.1, bf16[512,512]{1,0:T(8,128)(2,1)} %refs_1_.1, bf16[512,512]{1,0:T(8,128)(2,1)} %refs_2_.1, bf16[512,128]{1,0:T(8,128)(2,1)} %refs_3_.1, bf16[512,128]{1,0:T(8,128)(2,1)} %refs_4_.1, f32[8,512]{1,0:T(8,128)} %bitcast.10, f32[1,8]{1,0:T(1,128)} %bitcast.15, ...), custom_call_target="tpu_custom_call" | custom-call | tf_op jit(solution)/shard_map/pallas_call | solution.py:837
  98.5 1.9 %copy.24 = bf16[128,2048]{1,0:T(8,128)(2,1)} copy(bf16[128,2048]{1,0:T(8,128)(2,1)} %shard_map.208) | data formatting | bytes 1048576

commit v3 on v2

--- a/solution.py
+++ b/solution.py
@@ -341,14 +341,21 @@
         z_acc,
         to_row,
         incoming,
-        mix_out,
-        mix_far,
-        mix_in,
+        gated,
+        far_rows,
+        near_rows,
+        far_out,
+        far_got,
+        mixed,
+        w_near,
         nall,
+        tail_out,
+        tail_in,
         gu,
         ffn_out,
-        ffn_far,
+        ffn_far_in,
         ffn_in,
+        ffn_mixed,
         send_sem,
         gather_sem,
         pair_sem,
@@ -357,6 +364,7 @@
         z_sem,
         back_sem,
         mix_sem,
+        near_sem,
         all_sem,
         ffn_sem,
     ) = refs
@@ -407,6 +415,28 @@
         wire.send(src.at[last], dst, rank_dev(after), rim_sem.at[k], when=has_next)
     gather = weight_gather(wire, wv, gather_sem, pair_sem, ids, mark)
     gather(("start",))
+    w_source = sources[LOADED.index("w_mix")]
+
+    def w_rows(core, k):
+        return pl.ds(pl.multiple_of(core * 256 + k * 64, 64), 64)
+
+    for k in range(4):
+        for d, dev in enumerate((right, left)):
+            rows_k = w_rows(c, k)
+            wire.send(w_source.at[rows_k], w_near.at[d, rows_k], dev, near_sem.at[d, k])
+
+    def pass_on(k):
+        mark("w_pass" + str(k))
+        for d, dev in enumerate((left, right)):
+            v = w_near.at[d, w_rows(c, k)]
+            wire.arrive(v, near_sem.at[d, k], dev)
+            wire.send(v, v, {"sp_2": 1 - c}, near_sem.at[2 + d, k])
+
+    def w_whole():
+        mark("w_whole")
+        for k in range(4):
+            for d in range(2):
+                wire.arrive(w_near.at[d, w_rows(1 - c, k)], near_sem.at[2 + d, k], {"sp_2": 1 - c})
 
     rows_at = lax.broadcasted_iota(jnp.int32, (BLOCK, BLOCK), 0)
     cols_at = lax.broadcasted_iota(jnp.int32, (BLOCK, BLOCK), 1)
@@ -446,7 +476,6 @@
         b_act = conv_block(b_in, b_rim, b_taps, b).astype(BF16)
         xs[span] = x_act
         bs[span] = b_act
-        cs[span] = conv_block(c_in, c_rim, c_taps, b).astype(BF16)
         raw = deltas[:, span] + offset_col
         step_rows = jnp.maximum(raw, 0.0) + jnp.log1p(jnp.exp(-jnp.abs(raw)))
         cum_rows = spread(fading[:, span] - speed_col * step_rows, triu)
@@ -455,12 +484,16 @@
         both = jnp.concatenate([both, jnp.zeros((112, BLOCK), F32)], axis=0).T
         cums[span] = both
         cum, step = both[:, 0:HEADS], both[:, HEADS : 2 * HEADS]
-        grown = spread(jnp.exp(cum), onehot)
-        ec[span] = grown
+        grown = spread(jnp.broadcast_to(jnp.exp(cum[BLOCK - 1 : BLOCK]), (8, HEADS)), onehot)
         to_end = spread(step * jnp.exp(cum[BLOCK - 1 : BLOCK] - cum), onehot)
         weighted = (x_act.astype(F32) * to_end).astype(BF16)
         states[b] = dot(b_act.astype(F32).T.astype(BF16), weighted)
-        decays[b] = jnp.broadcast_to(grown[BLOCK - 1 : BLOCK], (8, INNER))
+        decays[b] = grown
+
+    def readout_block(b):
+        span = slice(b * BLOCK, (b + 1) * BLOCK)
+        cs[span] = conv_block(c_in, c_rim, c_taps, b).astype(BF16)
+        ec[span] = spread(jnp.exp(cums[span, 0:HEADS]), onehot)
 
     def within_block(b):
         span = slice(b * BLOCK, (b + 1) * BLOCK)
@@ -492,7 +525,6 @@
     mark("local2")
     local_block(2)
     local_block(1)
-    gather(("row_far",))
     mark("rim_wait")
 
     @pl.when(has_last)
@@ -529,8 +561,10 @@
         wire.send(own_decay, row_decay.at[place], row_dev(to), row_sem.at[1, k])
     row_ends[place] = ends[sixteen(place), :]
     row_decay[place] = own_decay[...]
-    gather(("x_send", 0), ("z_piece", 1))
+    gather(("row_far",), ("x_send", 0), ("z_piece", 1))
     mark("within01")
+    readout_block(0)
+    readout_block(1)
     within_block(0)
     within_block(1)
     mark("row_wait")
@@ -538,6 +572,7 @@
         src = wrap(place - k, 8)
         wire.arrive(row_ends.at[src], row_sem.at[0, k], row_dev(src))
         wire.arrive(row_decay.at[src], row_sem.at[1, k], row_dev(src))
+    pass_on(0)
     mark("row_fold")
     total = jnp.zeros((16, INNER), F32)
     growth = jnp.ones((1, INNER), F32)
@@ -553,8 +588,10 @@
         to = {"sp_0": wrap(z + k, 8)}
         wire.send(z_out, z_state.at[k], to, z_sem.at[0, k], when=z + k < 8)
         wire.send(z_dout, z_decay.at[k], to, z_sem.at[1, k], when=z + k < 8)
-    gather(("row_done",))
+    gather(("x_send", -1), ("row_done",))
     mark("within23")
+    readout_block(2)
+    readout_block(3)
     within_block(2)
     within_block(3)
     mark("z_wait")
@@ -576,7 +613,7 @@
         to = wrap(place + k, 8)
         wire.send(to_row.at[to], incoming.at[sixteen(place)], row_dev(to), back_sem.at[k])
     incoming[sixteen(place), :] = to_row[place]
-    gather(("x_send", -1), ("x_send", 1), ("x_piece", 0), ("z_piece", 2))
+    gather(("x_send", 1), ("x_piece", 0), ("z_piece", 2))
     mark("back_wait")
     for k in range(1, 8):
         src = wrap(place - k, 8)
@@ -586,79 +623,56 @@
         copy.wait()
     turns = [wrap(y + 2, 4), wrap(y + 1, 4), wrap(y - 1, 4), y]
 
-    def reduce_rows(part, sent, far, got, sems, fill, name):
-        upper, lower = pl.ds(0, 64), pl.ds(64, 64)
-        tiles = [pl.ds(j * 512, 512) for j in range(4)]
-        mark(name + "_part0")
-        tile = part(0)
-        for j, lanes in enumerate(tiles):
-            tile(j)
-            wire.send(sent.at[0, upper, lanes], far.at[0, :, lanes], right, sems.at[j])
-            wire.send(sent.at[0, lower, lanes], far.at[1, :, lanes], left, sems.at[4 + j])
-        mark(name + "_part1")
-        tile = part(1)
-        for j in range(4):
-            tile(j)
-        wire.send(sent.at[1, lower], got.at[0, lower], right, sems.at[8])
-        mark(name + "_part2")
-        tile = part(2)
-        for j in range(4):
-            tile(j)
-        wire.send(sent.at[2, upper], got.at[1, upper], left, sems.at[9])
-        fill(0)
-        mark(name + "_far_wait")
-        for j, lanes in enumerate(tiles):
-            at = slice(j * 512, (j + 1) * 512)
-            wire.arrive(far.at[0, :, lanes], sems.at[j], left)
-            sent[1, 0:64, at] = (sent[1, 0:64, at].astype(F32) + far[0, :, at].astype(F32)).astype(
-                BF16
-            )
-            wire.send(sent.at[1, upper, lanes], got.at[0, upper, lanes], right, sems.at[10 + j])
-            wire.arrive(far.at[1, :, lanes], sems.at[4 + j], right)
-            sent[2, 64:, at] = (sent[2, 64:, at].astype(F32) + far[1, :, at].astype(F32)).astype(
-                BF16
-            )
-            wire.send(sent.at[2, lower, lanes], got.at[1, lower, lanes], left, sems.at[14 + j])
-        fill(1)
-        mark(name + "_part3")
-        tile = part(3)
-        for j in range(4):
-            tile(j)
-        fill(2)
-        mark(name + "_wait")
-        wire.arrive(got.at[0, lower], sems.at[8], left)
-        wire.arrive(got.at[1, upper], sems.at[9], right)
-        for j, lanes in enumerate(tiles):
-            wire.arrive(got.at[0, upper, lanes], sems.at[10 + j], left)
-            wire.arrive(got.at[1, lower, lanes], sems.at[14 + j], right)
-        return sent[3].astype(F32) + got[0].astype(F32) + got[1].astype(F32)
-
-    def mix_part(k):
-        t = turns[k]
+    def gated_block(t):
         span = pl.ds(pl.multiple_of(t * BLOCK, BLOCK), BLOCK)
         begin = states[t] + incoming[...].astype(F32) * decays[t, 0:1]
         gated = yw[span, :] + ec[span, :] * dot(cs[span, :], begin.astype(BF16))
         gated = gated * silu(valve[span, :].astype(F32))
         gated = gated * lax.rsqrt(jnp.mean(gated * gated, axis=-1, keepdims=True) + EPSILON)
-        y_norm = (gated * cluster[...]).astype(BF16)
-
-        def tile(j):
-            lanes = slice(j * 512, (j + 1) * 512)
-            mix_out[k, :, lanes] = dot(y_norm, w_mix[:, lanes]).astype(BF16)
-
-        return tile
-
-    def mix_fill(stage):
-        if stage == 0:
-            gather(("x_send", -2), ("x_send", 2), ("z_group", 1, 0, 1), ("x_piece", -1), ("z_group", 1, 2, 3))
-        elif stage == 1:
-            gather(("z_piece", 3), ("x_piece", 1), ("x_send", -3), ("x_send", 3))
-        else:
-            gather(("x_piece", -2), ("x_piece", 2), ("x_far", 0))
-            gather(("z_group", 2, 0, 1), ("z_piece", 4), ("z_group", 2, 2, 3), ("x_send", 4), ("x_far", -1), ("x_far", 1))
-
-    mixer = reduce_rows(mix_part, mix_out, mix_far, mix_in, mix_sem, mix_fill, "mix")
+        return (gated * cluster[...]).astype(BF16)
+
+    mark("mix_blocks")
+    gated[0] = gated_block(turns[0])
+    wire.send(gated.at[0, pl.ds(0, 64)], far_rows.at[0], right, mix_sem.at[0])
+    wire.send(gated.at[0, pl.ds(64, 64)], far_rows.at[1], left, mix_sem.at[1])
+    gated[1] = gated_block(turns[1])
+    wire.send(gated.at[1], near_rows.at[0], right, mix_sem.at[2])
+    gated[2] = gated_block(turns[2])
+    wire.send(gated.at[2], near_rows.at[1], left, mix_sem.at[3])
+    pass_on(1)
+    pass_on(2)
+    mark("mix_own")
+    mixed[...] = dot(gated_block(y), w_mix[...])
+    gather(("x_send", -2), ("x_send", 2), ("z_group", 1, 0, 1), ("x_piece", -1), ("z_group", 1, 2, 3))
+    pass_on(3)
+    w_whole()
+    mark("mix_far_wait")
+    wire.arrive(far_rows.at[0], mix_sem.at[0], left)
+    wire.arrive(far_rows.at[1], mix_sem.at[1], right)
+    mark("mix_far")
+    for j in range(4):
+        lanes = pl.ds(j * 512, 512)
+        for d, dev in enumerate((right, left)):
+            far_out[d, :, j * 512 : (j + 1) * 512] = dot(
+                far_rows[d], w_near[d, :, j * 512 : (j + 1) * 512]
+            ).astype(BF16)
+            wire.send(far_out.at[d, :, lanes], far_got.at[d, :, lanes], dev, mix_sem.at[4 + 4 * d + j])
+    gather(("z_piece", 3), ("x_piece", 1), ("x_send", -3), ("x_send", 3))
+    mark("mix_near_wait")
+    wire.arrive(near_rows.at[0], mix_sem.at[2], left)
+    wire.arrive(near_rows.at[1], mix_sem.at[3], right)
+    mark("mix_near")
+    for d in range(2):
+        mixed[...] += dot(near_rows[d], w_near[d])
+    gather(("x_piece", -2), ("x_far", 0))
+    mark("mix_wait")
+    for j in range(4):
+        lanes = pl.ds(j * 512, 512)
+        for d, dev in enumerate((left, right)):
+            wire.arrive(far_got.at[d, :, lanes], mix_sem.at[4 + 4 * d + j], dev)
     mark("norm_one")
+    far_sum = jnp.concatenate([far_got[0], far_got[1]], axis=0).astype(F32)
+    mixer = mixed[...] + far_sum
     normed = layer_norm(ALPHA * resid[...].astype(F32) + mixer, scale_one[...]).astype(BF16)
 
     def chunk(t):
@@ -668,20 +682,23 @@
         return pl.ds(pl.multiple_of(16 + t * BLOCK + h * 64, 16), 64)
 
     nall[chunk(y), :] = normed
+    tail = normed[BLOCK - 16 :].astype(F32)[14:16]
+    tail_out[...] = jnp.concatenate(
+        [tail[:, k * 128 : (k + 1) * 128] for k in range(16)], axis=0
+    ).astype(BF16)
+    for k in range(4):
+        wire.send(
+            tail_out,
+            tail_in,
+            rank_dev(after, k),
+            all_sem.at[3, 0],
+            when=jnp.logical_and(has_next, y == 3),
+        )
     mark("all_send")
     for h in range(2):
         for dev, half_of in ((right, h), (left, 1 - h)):
             v = nall.at[chunk_half(y, half_of)]
             wire.send(v, v, dev, all_sem.at[0 if dev is right else 1, half_of])
-    for k in range(4):
-        wire.send(
-            nall.at[pl.ds(pl.multiple_of(y * BLOCK + BLOCK, 16), 16)],
-            nall.at[pl.ds(0, 16)],
-            rank_dev(after, k),
-            all_sem.at[3, 0],
-            when=jnp.logical_and(has_next, y == 3),
-        )
-
     def project(spans, offs, first, last_of):
         zs = [wrap(z + off, 8) for off in offs]
         deep = [pl.ds(pl.multiple_of(zz * 256, 256), 256) for zz in zs]
@@ -702,14 +719,89 @@
                 gu[span, lanes] = mine.astype(BF16).astype(F32) if last_of else mine
 
     far_t, right_t, left_t = turns[0], turns[1], turns[2]
-    whole, inner, outer = range(8), (0, 1, -1), (2, -2)
+    def hidden_rows(pieces):
+        columns = []
+        for j in range(11):
+            lanes = slice(j * 128, (j + 1) * 128)
+            up_lanes = slice(FF + j * 128, FF + (j + 1) * 128)
+            rows = []
+            for t, first, count in pieces:
+                at = pl.ds(pl.multiple_of(t * BLOCK + first + 8, 8), count + 8)
+                sums = []
+                for source, taps in ((lanes, gate_taps), (up_lanes, up_taps)):
+                    window = gu[at, source]
+                    weights = taps[:, lanes].astype(F32)
+                    total = weights[0:1] * window[6 : 6 + count]
+                    for k in range(1, 3):
+                        total = total + weights[k : k + 1] * window[6 + k : 6 + k + count]
+                    sums.append(total)
+                rows.append((silu(sums[0]) * sums[1]).astype(BF16))
+            columns.append(rows[0] if len(rows) == 1 else jnp.concatenate(rows, axis=0))
+        return jnp.concatenate(columns, axis=1)
+
+    def down(hidden, j):
+        w = wv[2 * j : 2 * j + 2, :, :, :, 2 * FF :].reshape(512, FF)
+        return lax.dot_general(hidden, w, NT, preferred_element_type=F32)
+
+    upper, lower = pl.ds(0, 64), pl.ds(64, 64)
+    tiles = [(j, pl.ds(j * 512, 512), slice(j * 512, (j + 1) * 512)) for j in range(4)]
+
+    def ffn_near():
+        mark("ffn_near")
+        hidden = hidden_rows(((right_t, 0, 64), (left_t, 64, 64)))
+        for j, lanes, at in tiles:
+            ffn_out[0, :, at] = down(hidden, j).astype(BF16)
+            wire.send(ffn_out.at[0, upper, lanes], ffn_in.at[0, upper, lanes], right, ffn_sem.at[j])
+            wire.send(
+                ffn_out.at[0, lower, lanes], ffn_in.at[1, lower, lanes], left, ffn_sem.at[4 + j]
+            )
+
+    def ffn_far():
+        mark("ffn_far")
+        hidden = hidden_rows(((far_t, 0, 128),))
+        for j, lanes, at in tiles:
+            ffn_out[1, :, at] = down(hidden, j).astype(BF16)
+            wire.send(ffn_out.at[1, lower, lanes], ffn_far_in.at[0, :, lanes], right, ffn_sem.at[8 + j])
+            wire.send(ffn_out.at[1, upper, lanes], ffn_far_in.at[1, :, lanes], left, ffn_sem.at[12 + j])
+
+    def ffn_last():
+        mark("ffn_mixed")
+        hidden = hidden_rows(((right_t, 64, 64), (left_t, 0, 64)))
+        for j, lanes, at in tiles:
+            ffn_mixed[:, at] = down(hidden, j)
+        mark("ffn_far_wait")
+        for j, lanes, at in tiles:
+            wire.arrive(ffn_far_in.at[0, :, lanes], ffn_sem.at[8 + j], left)
+            wire.arrive(ffn_far_in.at[1, :, lanes], ffn_sem.at[12 + j], right)
+            both = jnp.concatenate([ffn_far_in[0, :, at], ffn_far_in[1, :, at]], axis=0)
+            ffn_out[2, :, at] = (ffn_mixed[:, at] + both.astype(F32)).astype(BF16)
+            wire.send(
+                ffn_out.at[2, upper, lanes], ffn_in.at[0, lower, lanes], right, ffn_sem.at[16 + j]
+            )
+            wire.send(
+                ffn_out.at[2, lower, lanes], ffn_in.at[1, upper, lanes], left, ffn_sem.at[20 + j]
+            )
+        mark("ffn_own")
+        hidden = hidden_rows(((y, 0, 128),))
+        for j, lanes, at in tiles:
+            ffn_mixed[:, at] = down(hidden, j)
+        mark("ffn_wait")
+        for j, lanes, at in tiles:
+            wire.arrive(ffn_in.at[0, upper, lanes], ffn_sem.at[j], left)
+            wire.arrive(ffn_in.at[1, lower, lanes], ffn_sem.at[4 + j], right)
+            wire.arrive(ffn_in.at[0, lower, lanes], ffn_sem.at[16 + j], left)
+            wire.arrive(ffn_in.at[1, upper, lanes], ffn_sem.at[20 + j], right)
+        mark("norm_two")
+        return ffn_mixed[...] + ffn_in[0].astype(F32) + ffn_in[1].astype(F32)
+
+    inner, outer = (0, 1, -1), (2, -2)
     rest = (3, -3, 4)
-    gather(("x_piece", -3), ("pair_done", 0), ("pair_done", 1), ("pair_done", -1))
+    gather(("x_piece", 2), ("z_group", 2, 0, 1), ("z_piece", 4), ("x_send", 4))
+    gather(("z_group", 2, 2, 3), ("x_far", -1), ("x_far", 1), ("x_piece", -3))
+    gather(("pair_done", 0), ("pair_done", 1), ("pair_done", -1))
     own = (chunk(y),)
     mark("project_own")
     project(own, inner, True, False)
-    gather(("x_piece", 3), ("x_far", -2), ("x_far", 2), ("z_group", 3, 0, 1, 2, 3))
-    gather(("x_piece", 4))
     mark("all_first")
     v = nall.at[chunk_half(left_t, 0)]
     wire.arrive(v, all_sem.at[0, 0], left)
@@ -717,62 +809,41 @@
     v = nall.at[chunk_half(right_t, 1)]
     wire.arrive(v, all_sem.at[1, 1], right)
     wire.send(v, v, left, all_sem.at[2, 1])
-    gather(("x_far", -3), ("x_far", 3), ("pair_done", 2), ("pair_done", -2))
+    gather(("x_piece", 3), ("x_far", -2), ("x_far", 2), ("z_group", 3, 0, 1, 2, 3))
+    gather(("x_piece", 4), ("pair_done", 2), ("pair_done", -2))
     mark("project_own2")
     project(own, outer, False, False)
-    gather(("x_far", 4),)
+    gather(("x_far", -3),)
     mark("near_wait")
     wire.arrive(nall.at[chunk_half(left_t, 1)], all_sem.at[0, 1], left)
     wire.arrive(nall.at[chunk_half(right_t, 0)], all_sem.at[1, 0], right)
-    near = (chunk(left_t), chunk(right_t))
+
+    @pl.when(has_last)
+    def _():
+        wire.arrive(tail_in, all_sem.at[3, 0], rank_dev(before, 3))
+
+    @pl.when(jnp.logical_not(has_last))
+    def _():
+        tail_in[...] = jnp.zeros_like(tail_in)
+
+    rim = tail_in[...].astype(F32)
+    rim = jnp.concatenate([rim[2 * k : 2 * k + 2] for k in range(16)], axis=1)
+    nall[0:16] = jnp.concatenate([jnp.zeros((14, D), F32), rim], axis=0).astype(BF16)
+    near = (chunk(left_t), chunk(right_t), pl.ds(0, 16))
     mark("project_near")
     project(near, inner + outer, True, False)
-    gather(("z_group", 4, 0, 1, 2, 3), ("pair_done", 3), ("pair_done", -3), ("pair_done", 4))
+    gather(("x_far", 3), ("z_group", 4, 0, 1, 2, 3), ("x_far", 4))
+    gather(("pair_done", 3), ("pair_done", -3), ("pair_done", 4))
     mark("project_rest")
     project(own + near, rest, False, True)
+    ffn_near()
     mark("far_wait")
     wire.arrive(nall.at[chunk_half(far_t, 0)], all_sem.at[2, 0], left)
     wire.arrive(nall.at[chunk_half(far_t, 1)], all_sem.at[2, 1], right)
-    mark("halo")
-
-    @pl.when(has_last)
-    def _():
-        wire.arrive(nall.at[pl.ds(0, 16)], all_sem.at[3, 0], rank_dev(before, 3))
-
-    @pl.when(jnp.logical_not(has_last))
-    def _():
-        nall[0:16] = jnp.zeros((16, D), BF16)
     mark("project_far")
-    project((chunk(far_t), pl.ds(0, 16)), whole, True, True)
-
-    def conv_gu(t, lanes, taps, tap_lanes):
-        window = gu[pl.ds(pl.multiple_of(t * BLOCK + 8, 8), BLOCK + 8), lanes]
-        weights = taps[:, tap_lanes].astype(F32)
-        total = weights[0:1] * window[6 : 6 + BLOCK]
-        for k in range(1, 3):
-            total = total + weights[k : k + 1] * window[6 + k : 6 + k + BLOCK]
-        return total
-
-    def ffn_part(k):
-        t = turns[k]
-        pieces = []
-        for j in range(11):
-            lanes = slice(j * 128, (j + 1) * 128)
-            shifted_lanes = slice(FF + j * 128, FF + (j + 1) * 128)
-            gate = conv_gu(t, lanes, gate_taps, lanes)
-            pieces.append((silu(gate) * conv_gu(t, shifted_lanes, up_taps, lanes)).astype(BF16))
-        hidden = jnp.concatenate(pieces, axis=1)
-
-        def tile(j):
-            w = wv[2 * j : 2 * j + 2, :, :, :, 2 * FF :].reshape(512, FF)
-            ffn_out[k, :, j * 512 : (j + 1) * 512] = lax.dot_general(
-                hidden, w, NT, preferred_element_type=F32
-            ).astype(BF16)
-
-        return tile
-
-    channel = reduce_rows(ffn_part, ffn_out, ffn_far, ffn_in, ffn_sem, lambda stage: None, "ffn")
-    mark("norm_two")
+    project((chunk(far_t),), (0, 1, -1, 2, -2, 3, -3, 4), True, True)
+    ffn_far()
+    channel = ffn_last()
     out[...] = layer_norm(
         ALPHA * nall[chunk(y), :].astype(F32) + channel, scale_two[...]
     ).astype(BF16)
@@ -815,14 +886,21 @@
         pltpu.VMEM((16, INNER), F32),
         pltpu.VMEM((8, 16, INNER), BF16),
         pltpu.VMEM((STATE, INNER), BF16),
-        pltpu.VMEM((4, BLOCK, D), BF16),
+        pltpu.VMEM((3, BLOCK, INNER), BF16),
+        pltpu.VMEM((2, 64, INNER), BF16),
+        pltpu.VMEM((2, BLOCK, INNER), BF16),
+        pltpu.VMEM((2, 64, D), BF16),
+        pltpu.VMEM((2, 64, D), BF16),
+        pltpu.VMEM((BLOCK, D), F32),
+        pltpu.VMEM((2, INNER, D), BF16),
+        pltpu.VMEM((ROWS + 16, D), BF16),
+        pltpu.VMEM((32, 128), BF16),
+        pltpu.VMEM((32, 128), BF16),
+        pltpu.VMEM((ROWS + 16, 2 * FF), F32),
+        pltpu.VMEM((3, BLOCK, D), BF16),
         pltpu.VMEM((2, 64, D), BF16),
         pltpu.VMEM((2, BLOCK, D), BF16),
-        pltpu.VMEM((ROWS + 16, D), BF16),
-        pltpu.VMEM((ROWS + 16, 2 * FF), F32),
-        pltpu.VMEM((4, BLOCK, D), BF16),
-        pltpu.VMEM((2, 64, D), BF16),
-        pltpu.VMEM((2, BLOCK, D), BF16),
+        pltpu.VMEM((BLOCK, D), F32),
         dma((260,)),
         dma((86,)),
         dma((8,)),
@@ -830,9 +908,10 @@
         dma((2, 8)),
         dma((2, 8)),
         dma((8,)),
-        dma((18,)),
+        dma((12,)),
+        dma((4, 4)),
         dma((4, 2)),
-        dma((18,)),
+        dma((24,)),
     ]
     return pl.pallas_call(
         layer_kernel,
@@ -844,7 +923,6 @@
             collective_id=0, has_side_effects=True, vmem_limit_bytes=67043328
         ),
     )(*arrays)
-
 
 def solution(mesh):
     split = Mesh(mesh.devices.reshape(8, 4, 2, mesh.shape["tp"]), ("sp_0", "sp_1", "sp_2", "tp"))

time: 100 us -> 95.1 us (0.951)
  Pallas kernels: 98.5 us -> 93.1 us
    pallas_call x1, Pallas kernels: 98.5 us -> 93.1 us  [shards(): pl.pallas_call(layer_kernel, out_shape=jax.ShapeDtypeStruct((BLOCK, D), B...]
where the time goes in v3:
time: 95.1 us; the launch traced here: 95 us
  Pallas kernels  93.1 us (98%)
  local copies, waits for them, and re-layouts  1.88 us (2%)
    pallas_call x1, Pallas kernels, shards(): pl.pallas_call(layer_kernel, out_shape=jax.ShapeDtypeStruct((BLOCK, D), B...  93.1 us

profile of v3, /device:TPU:1, one launch (start us, length us, event | category | flops | bytes accessed | tf_op | source)
XLA Modules:
  0.0 95.0 jit_solution(16202620450251151884)
XLA Ops:
  0.0 93.1 %shard_map.208 = bf16[128,2048]{1,0:T(8,128)(2,1)} custom-call(bf16[128,2048]{1,0:T(8,128)(2,1)} %refs_0_.1, bf16[512,512]{1,0:T(8,128)(2,1)} %refs_1_.1, bf16[512,512]{1,0:T(8,128)(2,1)} %refs_2_.1, bf16[512,128]{1,0:T(8,128)(2,1)} %refs_3_.1, bf16[512,128]{1,0:T(8,128)(2,1)} %refs_4_.1, f32[8,512]{1,0:T(8,128)} %bitcast.10, f32[1,8]{1,0:T(1,128)} %bitcast.15, ...), custom_call_target="tpu_custom_call" | custom-call | tf_op jit(solution)/shard_map/pallas_call | solution.py:916
  93.1 1.9 %copy.24 = bf16[128,2048]{1,0:T(8,128)(2,1)} copy(bf16[128,2048]{1,0:T(8,128)(2,1)} %shard_map.208) | data formatting | bytes 1048576

commit v4 on v3

--- a/solution.py
+++ b/solution.py
@@ -588,7 +588,7 @@
         to = {"sp_0": wrap(z + k, 8)}
         wire.send(z_out, z_state.at[k], to, z_sem.at[0, k], when=z + k < 8)
         wire.send(z_dout, z_decay.at[k], to, z_sem.at[1, k], when=z + k < 8)
-    gather(("x_send", -1), ("row_done",))
+    gather(("x_send", -1), ("row_done",), ("z_group", 1, 0))
     mark("within23")
     readout_block(2)
     readout_block(3)
@@ -613,7 +613,7 @@
         to = wrap(place + k, 8)
         wire.send(to_row.at[to], incoming.at[sixteen(place)], row_dev(to), back_sem.at[k])
     incoming[sixteen(place), :] = to_row[place]
-    gather(("x_send", 1), ("x_piece", 0), ("z_piece", 2))
+    gather(("x_send", 1), ("x_piece", 0), ("z_piece", 2), ("z_group", 1, 1))
     mark("back_wait")
     for k in range(1, 8):
         src = wrap(place - k, 8)
@@ -643,7 +643,7 @@
     pass_on(2)
     mark("mix_own")
     mixed[...] = dot(gated_block(y), w_mix[...])
-    gather(("x_send", -2), ("x_send", 2), ("z_group", 1, 0, 1), ("x_piece", -1), ("z_group", 1, 2, 3))
+    gather(("x_send", -2), ("x_send", 2), ("x_piece", -1), ("z_group", 1, 2, 3))
     pass_on(3)
     w_whole()
     mark("mix_far_wait")
@@ -664,7 +664,8 @@
     mark("mix_near")
     for d in range(2):
         mixed[...] += dot(near_rows[d], w_near[d])
-    gather(("x_piece", -2), ("x_far", 0))
+    gather(("x_piece", -2), ("x_far", 0), ("x_piece", 2), ("z_group", 2, 0, 1))
+    gather(("z_piece", 4), ("x_send", 4))
     mark("mix_wait")
     for j in range(4):
         lanes = pl.ds(j * 512, 512)
@@ -784,24 +785,29 @@
         mark("ffn_own")
         hidden = hidden_rows(((y, 0, 128),))
         for j, lanes, at in tiles:
-            ffn_mixed[:, at] = down(hidden, j)
+            ffn_mixed[:, at] = down(hidden, j) + ALPHA * nall[chunk(y), at].astype(F32)
         mark("ffn_wait")
         for j, lanes, at in tiles:
             wire.arrive(ffn_in.at[0, upper, lanes], ffn_sem.at[j], left)
             wire.arrive(ffn_in.at[1, lower, lanes], ffn_sem.at[4 + j], right)
+        ffn_mixed[0:64] += ffn_in[0, 0:64].astype(F32)
+        ffn_mixed[64:] += ffn_in[1, 64:].astype(F32)
+        wire.finish()
+        for j, lanes, at in tiles:
             wire.arrive(ffn_in.at[0, lower, lanes], ffn_sem.at[16 + j], left)
             wire.arrive(ffn_in.at[1, upper, lanes], ffn_sem.at[20 + j], right)
         mark("norm_two")
-        return ffn_mixed[...] + ffn_in[0].astype(F32) + ffn_in[1].astype(F32)
+        last = jnp.concatenate([ffn_in[1, 0:64], ffn_in[0, 64:]], axis=0)
+        return ffn_mixed[...] + last.astype(F32)
 
     inner, outer = (0, 1, -1), (2, -2)
     rest = (3, -3, 4)
-    gather(("x_piece", 2), ("z_group", 2, 0, 1), ("z_piece", 4), ("x_send", 4))
     gather(("z_group", 2, 2, 3), ("x_far", -1), ("x_far", 1), ("x_piece", -3))
     gather(("pair_done", 0), ("pair_done", 1), ("pair_done", -1))
     own = (chunk(y),)
     mark("project_own")
     project(own, inner, True, False)
+    gather(("z_group", 3, 0, 1), ("x_piece", 3))
     mark("all_first")
     v = nall.at[chunk_half(left_t, 0)]
     wire.arrive(v, all_sem.at[0, 0], left)
@@ -809,8 +815,8 @@
     v = nall.at[chunk_half(right_t, 1)]
     wire.arrive(v, all_sem.at[1, 1], right)
     wire.send(v, v, left, all_sem.at[2, 1])
-    gather(("x_piece", 3), ("x_far", -2), ("x_far", 2), ("z_group", 3, 0, 1, 2, 3))
-    gather(("x_piece", 4), ("pair_done", 2), ("pair_done", -2))
+    gather(("x_far", -2), ("x_far", 2), ("z_group", 3, 2, 3), ("x_piece", 4))
+    gather(("pair_done", 2), ("pair_done", -2))
     mark("project_own2")
     project(own, outer, False, False)
     gather(("x_far", -3),)
@@ -835,8 +841,11 @@
     gather(("x_far", 3), ("z_group", 4, 0, 1, 2, 3), ("x_far", 4))
     gather(("pair_done", 3), ("pair_done", -3), ("pair_done", 4))
     mark("project_rest")
-    project(own + near, rest, False, True)
+    own_tail = pl.ds(pl.multiple_of(y * BLOCK + BLOCK, 16), 16)
+    project(near + (own_tail,), rest, False, True)
     ffn_near()
+    mark("project_own3")
+    project((pl.ds(pl.multiple_of(y * BLOCK + 16, 16), BLOCK - 16),), rest, False, True)
     mark("far_wait")
     wire.arrive(nall.at[chunk_half(far_t, 0)], all_sem.at[2, 0], left)
     wire.arrive(nall.at[chunk_half(far_t, 1)], all_sem.at[2, 1], right)
@@ -844,11 +853,7 @@
     project((chunk(far_t),), (0, 1, -1, 2, -2, 3, -3, 4), True, True)
     ffn_far()
     channel = ffn_last()
-    out[...] = layer_norm(
-        ALPHA * nall[chunk(y), :].astype(F32) + channel, scale_two[...]
-    ).astype(BF16)
-    mark("finish")
-    wire.finish()
+    out[...] = layer_norm(channel, scale_two[...]).astype(BF16)
     mark.end()
 
 

time: 95.1 us -> 92.1 us (0.968)
  Pallas kernels: 93.1 us -> 90 us
    pallas_call x1, Pallas kernels: 93.1 us -> 90 us  [shards(): pl.pallas_call(layer_kernel, out_shape=jax.ShapeDtypeStruct((BLOCK, D), B...]
where the time goes in v4:
time: 92.1 us; the launch traced here: 91.9 us
  Pallas kernels  90 us (98%)
  local copies, waits for them, and re-layouts  1.88 us (2%)
    pallas_call x1, Pallas kernels, shards(): pl.pallas_call(layer_kernel, out_shape=jax.ShapeDtypeStruct((BLOCK, D), B...  90 us
    unnamed x1, local copies, waits for them, and re-layouts  1.88 us

profile of v4, /device:TPU:1, one launch (start us, length us, event | category | flops | bytes accessed | tf_op | source)
XLA Modules:
  0.0 91.9 jit_solution(11834106609622969828)
XLA Ops:
  0.0 90.0 %shard_map.208 = bf16[128,2048]{1,0:T(8,128)(2,1)} custom-call(bf16[128,2048]{1,0:T(8,128)(2,1)} %refs_0_.1, bf16[512,512]{1,0:T(8,128)(2,1)} %refs_1_.1, bf16[512,512]{1,0:T(8,128)(2,1)} %refs_2_.1, bf16[512,128]{1,0:T(8,128)(2,1)} %refs_3_.1, bf16[512,128]{1,0:T(8,128)(2,1)} %refs_4_.1, f32[8,512]{1,0:T(8,128)} %bitcast.10, f32[1,8]{1,0:T(1,128)} %bitcast.15, ...), custom_call_target="tpu_custom_call" | custom-call | tf_op jit(solution)/shard_map/pallas_call | solution.py:921
  90.1 1.9 %copy.24 = bf16[128,2048]{1,0:T(8,128)(2,1)} copy(bf16[128,2048]{1,0:T(8,128)(2,1)} %shard_map.208) | data formatting | bytes 1048576

commit v5 on v4

--- a/solution.py
+++ b/solution.py
@@ -405,13 +405,14 @@
     copies += [pltpu.make_async_copy(sources[k], loads[k], load_sem.at[k]) for k in order]
     for copy in copies:
         copy.start()
-    for copy in copies[: 3 + len(EARLY)]:
+    for copy in copies[:3]:
         copy.wait()
     pl.semaphore_wait(sem, len(greeted))
 
     has_next, has_last = rank < 63, rank > 0
     last = pl.ds(ROWS - 16, 16)
-    for k, (src, dst) in enumerate(((x_in, x_rim), (b_in, b_rim), (c_in, c_rim))):
+    for k, dst in enumerate((x_rim, b_rim, c_rim)):
+        src = sources[LOADED.index(("x_in", "b_in", "c_in")[k])]
         wire.send(src.at[last], dst, rank_dev(after), rim_sem.at[k], when=has_next)
     gather = weight_gather(wire, wv, gather_sem, pair_sem, ids, mark)
     gather(("start",))
@@ -424,6 +425,9 @@
         for d, dev in enumerate((right, left)):
             rows_k = w_rows(c, k)
             wire.send(w_source.at[rows_k], w_near.at[d, rows_k], dev, near_sem.at[d, k])
+
+    for copy in copies[3 : 3 + len(EARLY)]:
+        copy.wait()
 
     def pass_on(k):
         mark("w_pass" + str(k))

time: 92.1 us -> 91.9 us (level)
  no operation moved by 1% of the time
where the time goes in v5:
time: 91.9 us; the launch traced here: 91.8 us
  Pallas kernels  89.9 us (98%)
  local copies, waits for them, and re-layouts  1.88 us (2%)
    pallas_call x1, Pallas kernels, shards(): pl.pallas_call(layer_kernel, out_shape=jax.ShapeDtypeStruct((BLOCK, D), B...  89.9 us
    unnamed x1, local copies, waits for them, and re-layouts  1.88 us

profile of v5, /device:TPU:1, one launch (start us, length us, event | category | flops | bytes accessed | tf_op | source)
XLA Modules:
  0.0 91.8 jit_solution(10902818257393209026)
XLA Ops:
  0.0 89.9 %shard_map.208 = bf16[128,2048]{1,0:T(8,128)(2,1)} custom-call(bf16[128,2048]{1,0:T(8,128)(2,1)} %refs_0_.1, bf16[512,512]{1,0:T(8,128)(2,1)} %refs_1_.1, bf16[512,512]{1,0:T(8,128)(2,1)} %refs_2_.1, bf16[512,128]{1,0:T(8,128)(2,1)} %refs_3_.1, bf16[512,128]{1,0:T(8,128)(2,1)} %refs_4_.1, f32[8,512]{1,0:T(8,128)} %bitcast.10, f32[1,8]{1,0:T(1,128)} %bitcast.15, ...), custom_call_target="tpu_custom_call" | custom-call | tf_op jit(solution)/shard_map/pallas_call | solution.py:925
  89.9 1.9 %copy.24 = bf16[128,2048]{1,0:T(8,128)(2,1)} copy(bf16[128,2048]{1,0:T(8,128)(2,1)} %shard_map.208) | data formatting | bytes 1048576
